TPU v7x, 256 devices: a whole 4x4x8 slice. The times are simulated.
256 devices in a mesh: tp: 32 (over z, x), dp: 8 (over y, core).
Axes of the slice: x: 4, y: 4, z: 8, core: 2. Of those that a mesh axis runs over, the one named last changes fastest.
Arguments:
- stream: bfloat16 [256, 4096], P(None, 'dp'), may hold values from -12 to 12
- history: int32 [256], P('dp'), may hold values from 1 to 4096, 262144 in all
- input_norm_gain: float32 [2, 4096], P(None, 'dp'), may hold values from 0.1 to 1.9
- query_weight: bfloat16 [2, 4096, 4096], P(None, 'dp', 'tp'), may hold values from -0.09375 to 0.09375
- key_weight: bfloat16 [2, 4096, 4096], P(None, 'dp', 'tp'), may hold values from -0.09375 to 0.09375
- value_weight: bfloat16 [2, 4096, 4096], P(None, 'dp', 'tp'), may hold values from -0.09375 to 0.09375
- gate_weight: bfloat16 [2, 4096, 4096], P(None, 'dp', 'tp'), may hold values from -0.09375 to 0.09375
- adapter_down_weight: bfloat16 [2, 4096, 128], P(None, 'dp'), may hold values from -0.09375 to 0.09375
- decay_up_weight: float32 [2, 64, 4096], P(None, None, 'tp'), may hold values from -3 to 3
- rate_up_weight: float32 [2, 64, 4096], P(None, None, 'tp'), may hold values from -3 to 3
- decay_offset: float32 [2, 4096], P(None, 'tp'), may hold values from -3 to 1
- head_norm_gain: float32 [2, 4096], P(None, 'tp'), may hold values from 0.1 to 1.9
- output_weight: bfloat16 [2, 4096, 4096], P(None, 'tp', 'dp'), may hold values from -0.09375 to 0.09375
- recurrent_state: float32 [2, 256, 64, 4096], P(None, 'dp', 'tp'), may hold values from -5 to 5
Outputs:
- stream_out: bfloat16 [256, 4096], P(None, 'dp')
- state_out: float32 [2, 256, 64, 4096], P(None, 'dp', 'tp')
All inputs are finite; a program needn't handle non-finite values. No bound on the sum of `history` on one device may be relied on, other than what follows from the above.
Results may differ from a plain program's by a relative error of at most 0.024.
Values may be sent and summed in bfloat16 or wider, within the bound.
A program may use at most 64 MiB of HBM per device.

v0:
```python
import math

import jax
import jax.numpy as jnp
from jax import lax
from jax.sharding import PartitionSpec as P

MODEL_WIDTH = 4096
HEAD = 64
ADAPTER_RANK = 64
SPAN = 64
BLOCK_COUNT = 2


NORM_EPS = 0.25
GROUP_EPS = 0.25


def split_up(array, dim, count):
    before, after = (array.shape[:dim], array.shape[dim + 1 :])
    return jnp.moveaxis(array.reshape(*before, count, -1, *after), dim, 0)


def summed_on_arrival(array, axis, dim):
    tiles = split_up(array, dim, lax.axis_size(axis))
    arrived = lax.all_to_all(tiles, axis, split_axis=0, concat_axis=0, tiled=True)
    return arrived.astype(jnp.float32).sum(axis=0)


def side_by_side(arrays, axis, dim, along):
    widths = [math.prod(a.shape[along:]) for a in arrays]
    both = jnp.concatenate(
        [a.reshape(*a.shape[:along], w) for a, w in zip(arrays, widths)], axis=along
    )
    whole = summed_on_arrival(both, axis, dim)
    tiles = jnp.split(whole, [sum(widths[:k]) for k in range(1, len(widths))], axis=along)
    return tuple((b.reshape(*whole.shape[:along], *a.shape[along:]) for a, b in zip(arrays, tiles)))


def laid_out(tiles, dim):
    tiles = jnp.moveaxis(tiles, 0, dim)
    shape = tiles.shape
    return tiles.reshape(*shape[:dim], shape[dim] * shape[dim + 1], *shape[dim + 2 :])


def sent_to_all(array, axis):
    count = lax.axis_size(axis)
    return lax.all_to_all(
        jnp.broadcast_to(array[None], (count, *array.shape)), axis, 0, 0, tiled=True
    )


def collect(array, axis, dim):
    return laid_out(sent_to_all(array, axis), dim)


def truncated_product(rescaled_rows, weight):
    product = jnp.dot(rescaled_rows, weight, preferred_element_type=jnp.float32).astype(
        jnp.bfloat16
    )
    return lax.optimization_barrier(product).astype(jnp.float32)


def recur_heads(
    query,
    key_proj,
    value_proj,
    gate_pre,
    adapter_hidden,
    pos_factor,
    decay_up_weight,
    rate_up_weight,
    decay_offset,
    head_norm_gain,
    recurrent_state,
):
    seq_local, width = query.shape
    head_count = width // HEAD
    decay_logits = decay_offset[None, :] + jnp.dot(
        jnp.tanh(adapter_hidden[:, :ADAPTER_RANK]), decay_up_weight
    )
    rate_log = -jax.nn.softplus(-decay_logits) - 0.5
    decay = jnp.exp(-jnp.exp(rate_log) * pos_factor)
    learning_rate = jax.nn.sigmoid(jnp.dot(adapter_hidden[:, ADAPTER_RANK:], rate_up_weight))

    def heads_of(values):
        return values.reshape(seq_local, head_count, HEAD)

    keys = heads_of(key_proj)
    key_unit = keys * lax.rsqrt(jnp.sum(keys * keys, axis=-1, keepdims=True) + 1.0)
    key_rate = key_unit * heads_of(learning_rate)
    matrix = recurrent_state.reshape(seq_local, head_count, HEAD, HEAD)
    state_key = jnp.einsum("bhvk,bhk->bhv", matrix, key_unit)
    refreshed_state = (
        matrix * heads_of(decay)[:, :, None, :]
        - state_key[..., None] * key_rate[:, :, None, :]
        + heads_of(value_proj)[..., None] * keys[:, :, None, :]
    )
    readout = jnp.einsum("bhvk,bhk->bhv", refreshed_state, heads_of(query))
    mean_y = jnp.mean(readout, axis=-1, keepdims=True)
    spread = jnp.mean(jnp.square(readout - mean_y), axis=-1, keepdims=True)
    normed = ((readout - mean_y) * lax.rsqrt(spread + GROUP_EPS)).reshape(
        seq_local, width
    ) * head_norm_gain[None, :]
    mixed = (normed * jax.nn.sigmoid(gate_pre)).astype(jnp.bfloat16)
    return (mixed, refreshed_state.reshape(seq_local, head_count, HEAD * HEAD))


def body(
    stream,
    history,
    input_norm_gain,
    query_weight,
    key_weight,
    value_weight,
    gate_weight,
    adapter_down_weight,
    decay_up_weight,
    rate_up_weight,
    decay_offset,
    head_norm_gain,
    output_weight,
    recurrent_state,
):
    pos_factor = (0.5 + (history // SPAN % 3).astype(jnp.float32))[:, None]
    new_states = []
    for layer_lookup in range(BLOCK_COUNT):
        widened = stream.astype(jnp.float32)
        squares = jnp.sum(widened * widened, axis=1)
        rescaled_rows = (widened * input_norm_gain[layer_lookup][None, :]).astype(jnp.bfloat16)
        query_part = truncated_product(rescaled_rows, query_weight[layer_lookup])
        key_part = truncated_product(rescaled_rows, key_weight[layer_lookup])
        value_part = truncated_product(rescaled_rows, value_weight[layer_lookup])
        gate_part = truncated_product(rescaled_rows, gate_weight[layer_lookup])
        adapter_section = truncated_product(rescaled_rows, adapter_down_weight[layer_lookup])
        high_part = lax.optimization_barrier(squares.astype(jnp.bfloat16)).astype(jnp.float32)
        low_part = lax.optimization_barrier((squares - high_part).astype(jnp.bfloat16)).astype(
            jnp.float32
        )
        joined = side_by_side(
            (
                query_part.astype(jnp.bfloat16),
                key_part.astype(jnp.bfloat16),
                value_part.astype(jnp.bfloat16),
                gate_part.astype(jnp.bfloat16),
                adapter_section.astype(jnp.bfloat16),
                high_part.astype(jnp.bfloat16),
                low_part.astype(jnp.bfloat16),
            ),
            "dp",
            0,
            1,
        )
        summed = joined[:5]
        own_sq = joined[5] + joined[6]
        inverse_root_mean = lax.rsqrt(own_sq / MODEL_WIDTH + NORM_EPS)[:, None]
        query, key_proj, value_proj, gate_pre, adapter_hidden = [
            part_sum * inverse_root_mean for part_sum in summed
        ]
        mixed, refreshed_state = recur_heads(
            query,
            key_proj,
            value_proj,
            gate_pre,
            adapter_hidden,
            pos_factor,
            decay_up_weight[layer_lookup],
            rate_up_weight[layer_lookup],
            decay_offset[layer_lookup],
            head_norm_gain[layer_lookup],
            recurrent_state[layer_lookup],
        )
        new_states.append(refreshed_state)
        out_weight = output_weight[layer_lookup]
        mixed_all = collect(mixed, "dp", 0)
        row_count = stream.shape[0] // lax.axis_size("tp")
        partial_value = summed_on_arrival(
            jnp.dot(mixed_all, out_weight, preferred_element_type=jnp.float32).astype(jnp.bfloat16),
            "tp",
            0,
        )
        own_rows = lax.dynamic_slice_in_dim(widened, lax.axis_index("tp") * row_count, row_count, 0)
        stream = collect((own_rows + partial_value).astype(jnp.bfloat16), "tp", 0)
    return (stream, jnp.stack(new_states))


def solution(mesh):
    placed = (
        P(None, "dp"),
        P("dp"),
        P(None, "dp"),
        P(None, "dp", "tp"),
        P(None, "dp", "tp"),
        P(None, "dp", "tp"),
        P(None, "dp", "tp"),
        P(None, "dp", None),
        P(None, None, "tp"),
        P(None, None, "tp"),
        P(None, "tp"),
        P(None, "tp"),
        P(None, "tp", "dp"),
        P(None, "dp", "tp", None),
    )
    return jax.shard_map(
        body,
        mesh=mesh,
        in_specs=placed,
        out_specs=(P(None, "dp"), P(None, "dp", "tp", None)),
        check_vma=False,
    )
```

profile of v0, /device:TPU:1, one launch (start us, length us, event | category | flops | bytes accessed | tf_op | source)
XLA Modules:
  0.0 186.7 jit_solution(9400263078024706563)
XLA Ops:
  9.8 6.6 %all-to-all-start = ((bf16[8,32,642]{2,1,0:T(8,128)(2,1)}), bf16[8,32,642]{2,1,0:T(8,128)(2,1)S(1)}, u32[]{:S(2)}, u32[]{:S(2)}) async-start(bf16[8,32,642]{2,1,0:T(8,128)(2,1)} %concatenate.43), calls=%async_computation | async-start | bytes 786432 | tf_op jit(solution)/shard_map/all_to_all | solution.py:26
  18.1 3.2 %reshape_squeeze.6 = f32[32,2,64,64]{3,2,1,0:T(8,128)} reshape(f32[1,32,2,4096]{3,2,1,0:T(2,128)} %get-tuple-element.9) | data formatting | bytes 2097152 | tf_op jit(solution)/shard_map/reshape;squeeze | solution.py:92
  21.8 2.2 %all-to-all-done = bf16[8,32,642]{2,1,0:T(8,128)(2,1)S(1)} async-done(((bf16[8,32,642]{2,1,0:T(8,128)(2,1)}), bf16[8,32,642]{2,1,0:T(8,128)(2,1)S(1)}, u32[]{:S(2)}, u32[]{:S(2)}) %all-to-all-start) | async-done | bytes 328736 | tf_op jit(solution)/shard_map/all_to_all | solution.py:26
  29.1 2.4 %fusion.104 = f32[32,2,1,64]{3,2,1,0:T(1,128)S(1)} fusion(f32[32,2,64,1]{2,3,1,0:T(1,128)S(1)} %bitcast.137, f32[32,2,64,64]{3,2,1,0:T(8,128)} %reshape_squeeze.6), kind=kOutput, calls=%fused_computation.170 | convolution fusion | flops 524288 | bytes 1081344 | tf_op jit(solution)/shard_map/bhvk,bhk->bhv/dot_general | solution.py:93
  35.7 8.4 %all_to_all.40 = bf16[8,32,128]{2,1,0:T(8,128)(2,1)S(1)} all-to-all(bf16[8,32,128]{2,1,0:T(8,128)(2,1)S(1)} %broadcast_in_dim.8), channel_id=1, replica_groups=mesh['tp'=32,'dp'=8] {'dp'}, dimensions={0} | all-to-all | bytes 131072 | tf_op jit(solution)/shard_map/all_to_all | solution.py:48
  44.1 1.8 fusion.8
  46.0 10.5 %all-to-all-start.2 = ((bf16[32,8,512]{2,1,0:T(8,128)(2,1)}), bf16[32,8,512]{2,1,0:T(8,128)(2,1)}, u32[]{:S(2)}, u32[]{:S(2)}) async-start(bf16[32,8,512]{2,1,0:T(8,128)(2,1)} %fusion.8), calls=%async_computation.2 | async-start | bytes 524288 | tf_op jit(solution)/shard_map/all_to_all | solution.py:26
  57.4 10.4 %all-to-all-done.2 = bf16[32,8,512]{2,1,0:T(8,128)(2,1)} async-done(((bf16[32,8,512]{2,1,0:T(8,128)(2,1)}), bf16[32,8,512]{2,1,0:T(8,128)(2,1)}, u32[]{:S(2)}, u32[]{:S(2)}) %all-to-all-start.2) | async-done | bytes 262176 | tf_op jit(solution)/shard_map/all_to_all | solution.py:26
  70.2 4.9 %all-to-all-start.3 = ((bf16[32,8,512]{2,1,0:T(8,128)(2,1)}), bf16[32,8,512]{2,1,0:T(8,128)(2,1)S(1)}, u32[]{:S(2)}, u32[]{:S(2)}) async-start(bf16[32,8,512]{2,1,0:T(8,128)(2,1)} %broadcast_in_dim.9), calls=%async_computation.3 | async-start | bytes 524288 | tf_op jit(solution)/shard_map/all_to_all | solution.py:48
  75.1 2.5 %reshape_squeeze.7 = f32[32,2,64,64]{3,2,1,0:T(8,128)} reshape(f32[1,32,2,4096]{3,2,1,0:T(2,128)S(1)} %get-tuple-element.8) | data formatting | bytes 2097152 | tf_op jit(solution)/shard_map/reshape;squeeze | solution.py:92
  77.6 7.9 %all-to-all-done.3 = bf16[32,8,512]{2,1,0:T(8,128)(2,1)S(1)} async-done(((bf16[32,8,512]{2,1,0:T(8,128)(2,1)}), bf16[32,8,512]{2,1,0:T(8,128)(2,1)S(1)}, u32[]{:S(2)}, u32[]{:S(2)}) %all-to-all-start.3) | async-done | bytes 262176 | tf_op jit(solution)/shard_map/all_to_all | solution.py:48
  91.9 7.7 %all-to-all-start.4 = ((bf16[8,32,642]{2,1,0:T(8,128)(2,1)}), bf16[8,32,642]{2,1,0:T(8,128)(2,1)}, u32[]{:S(2)}, u32[]{:S(2)}) async-start(bf16[8,32,642]{2,1,0:T(8,128)(2,1)} %concatenate.51), calls=%async_computation.4 | async-start | bytes 786432 | tf_op jit(solution)/shard_map/all_to_all | solution.py:26
  99.6 1.9 %broadcast_multiply_fusion.2 = f32[32,2,64,64]{3,2,1,0:T(8,128)} fusion(f32[32,2,64]{2,1,0:T(2,128)S(1)} %reshape.268, f32[32,2,64]{2,1,0:T(2,128)S(1)} %copy-done.9), kind=kLoop, calls=%fused_computation.40 | loop fusion | flops 262144 | bytes 1081344 | tf_op jit(solution)/shard_map/mul | solution.py:97
  101.5 2.4 %mul.399 = f32[1,32,2,4096]{3,2,1,0:T(2,128)S(1)} reshape(f32[32,2,64,64]{3,2,1,0:T(8,128)} %broadcast_multiply_fusion.2) | data formatting | bytes 2097152 | tf_op jit(solution)/shard_map/mul | solution.py:97
  105.5 3.2 %mul.396 = f32[1,32,2,4096]{3,2,1,0:T(2,128)} reshape(f32[32,2,64,64]{3,2,1,0:T(8,128)} %mul.341) | data formatting | bytes 2097152 | tf_op jit(solution)/shard_map/mul | solution.py:95
  108.7 1.9 %broadcast_multiply_fusion.3 = f32[32,2,64,64]{3,2,1,0:T(8,128)} fusion(f32[32,2,64]{2,1,0:T(2,128)S(1)} %copy-done.14, f32[32,2,64]{2,1,0:T(2,128)S(1)} %bitcast.134), kind=kLoop, calls=%fused_computation.41 | loop fusion | flops 262144 | bytes 1081344 | tf_op jit(solution)/shard_map/mul | solution.py:96
  110.6 3.2 %mul.398 = f32[1,32,2,4096]{3,2,1,0:T(2,128)} reshape(f32[32,2,64,64]{3,2,1,0:T(8,128)} %broadcast_multiply_fusion.3) | data formatting | bytes 2097152 | tf_op jit(solution)/shard_map/mul | solution.py:96
  123.7 2.2 %fusion.105 = f32[32,2,1,64]{3,2,1,0:T(1,128)S(1)} fusion(f32[32,2,64,1]{2,3,1,0:T(1,128)S(1)} %bitcast.138, f32[32,2,64,64]{3,2,1,0:T(8,128)} %reshape_squeeze.7), kind=kOutput, calls=%fused_computation.171 | convolution fusion | flops 524288 | bytes 1081344 | tf_op jit(solution)/shard_map/bhvk,bhk->bhv/dot_general | solution.py:93
  126.0 2.1 %fusion = f32[32,2,1,64]{3,2,1,0:T(1,128)} fusion(f32[32,2,64,1]{2,3,1,0:T(1,128)S(1)} %bitcast.150, f32[32,2,64,64]{3,2,1,0:T(8,128)S(1)} %copy-done.1, f32[32,2,64]{2,1,0:T(2,128)S(1)} %copy-done.10, f32[32,2,64]{2,1,0:T(2,128)S(1)} %get-tuple-element.2, f32[32,2,64]{2,1,0:T(2,128)S(1)} %bitcast.135, f32[32,2,64]{2,1,0:T(2,128)S(1)} %reshape.274, ...), kind=kOutput, calls=%fused_computation.1 | convolution fusion | flops 1835008 | bytes 1163264 | tf_op jit(solution)/shard_map/bhvk,bhk->bhv/dot_general | solution.py:99
  133.6 4.8 %all-to-all-start.5 = ((bf16[8,32,128]{2,1,0:T(8,128)(2,1)}), bf16[8,32,128]{2,1,0:T(8,128)(2,1)S(1)}, u32[]{:S(2)}, u32[]{:S(2)}) async-start(bf16[8,32,128]{2,1,0:T(8,128)(2,1)} %broadcast_in_dim.10), calls=%async_computation.5 | async-start | bytes 131072 | tf_op jit(solution)/shard_map/all_to_all | solution.py:48
  139.3 4.0 %all-to-all-done.5 = bf16[8,32,128]{2,1,0:T(8,128)(2,1)S(1)} async-done(((bf16[8,32,128]{2,1,0:T(8,128)(2,1)}), bf16[8,32,128]{2,1,0:T(8,128)(2,1)S(1)}, u32[]{:S(2)}, u32[]{:S(2)}) %all-to-all-start.5) | async-done | bytes 65568 | tf_op jit(solution)/shard_map/all_to_all | solution.py:48
  143.3 1.8 fusion.9
  145.1 4.1 %all-to-all-start.6 = ((bf16[32,8,512]{2,1,0:T(8,128)(2,1)}), bf16[32,8,512]{2,1,0:T(8,128)(2,1)S(1)}, u32[]{:S(2)}, u32[]{:S(2)}) async-start(bf16[32,8,512]{2,1,0:T(8,128)(2,1)} %fusion.9), calls=%async_computation.6 | async-start | bytes 524288 | tf_op jit(solution)/shard_map/all_to_all | solution.py:26
  149.2 2.7 %broadcast_multiply_fusion = f32[32,2,64,64]{3,2,1,0:T(8,128)} fusion(f32[32,2,64]{2,1,0:T(2,128)S(1)} %reshape.274, f32[32,2,64]{2,1,0:T(2,128)} %mul.384), kind=kLoop, calls=%fused_computation.37 | loop fusion | flops 262144 | bytes 1081344 | tf_op jit(solution)/shard_map/mul | solution.py:97
  151.9 3.2 %mul.403 = f32[1,32,2,4096]{3,2,1,0:T(2,128)} reshape(f32[32,2,64,64]{3,2,1,0:T(8,128)} %broadcast_multiply_fusion) | data formatting | bytes 2097152 | tf_op jit(solution)/shard_map/mul | solution.py:97
  155.1 1.9 %broadcast_multiply_fusion.1 = f32[32,2,64,64]{3,2,1,0:T(8,128)} fusion(f32[32,2,64]{2,1,0:T(2,128)S(1)} %copy-done.16, f32[32,2,64]{2,1,0:T(2,128)S(1)} %bitcast.136), kind=kLoop, calls=%fused_computation.38 | loop fusion | flops 262144 | bytes 1081344 | tf_op jit(solution)/shard_map/mul | solution.py:96
  157.0 3.2 %mul.402 = f32[1,32,2,4096]{3,2,1,0:T(2,128)} reshape(f32[32,2,64,64]{3,2,1,0:T(8,128)} %broadcast_multiply_fusion.1) | data formatting | bytes 2097152 | tf_op jit(solution)/shard_map/mul | solution.py:96
  161.7 3.2 %mul.400 = f32[1,32,2,4096]{3,2,1,0:T(2,128)} reshape(f32[32,2,64,64]{3,2,1,0:T(8,128)} %mul.373) | data formatting | bytes 2097152 | tf_op jit(solution)/shard_map/mul | solution.py:95
  166.3 9.0 %all-to-all-start.7 = ((bf16[32,8,512]{2,1,0:T(8,128)(2,1)}), bf16[32,8,512]{2,1,0:T(8,128)(2,1)S(1)}, u32[]{:S(2)}, u32[]{:S(2)}) async-start(bf16[32,8,512]{2,1,0:T(8,128)(2,1)} %broadcast_in_dim.11), calls=%async_computation.7 | async-start | bytes 524288 | tf_op jit(solution)/shard_map/all_to_all | solution.py:48
  175.4 4.9 %subtract_add_fusion.1 = (f32[1,32,2,4096]{3,2,1,0:T(2,128)S(1)}, f32[1,32,2,4096]{3,2,1,0:T(2,128)S(1)}) fusion(f32[1,32,2,4096]{3,2,1,0:T(2,128)S(1)} %mul.399, f32[1,32,2,4096]{3,2,1,0:T(2,128)} %mul.398, f32[1,32,2,4096]{3,2,1,0:T(2,128)} %mul.396, f32[2,32,2,4096]{3,2,1,0:T(2,128)S(1)} %copy-done, f32[1,32,2,4096]{3,2,1,0:T(2,128)} %mul.403, ...), kind=kLoop, calls=%fused_computation.36 | loop fusion | flops 1572864 | bytes 10485760 | tf_op jit(solution)/shard_map/add | solution.py:95
  180.3 2.4 %pad_maximum_fusion = f32[2,32,2,4096]{3,2,1,0:T(2,128)} fusion(f32[1,32,2,4096]{3,2,1,0:T(2,128)S(1)} %get-tuple-element.7, f32[1,32,2,4096]{3,2,1,0:T(2,128)S(1)} %get-tuple-element.6), kind=kLoop, calls=%fused_computation | loop fusion | flops 524288 | bytes 4194304 | tf_op jit(solution)/shard_map/stack | solution.py:184
  182.7 3.3 %all-to-all-done.7 = bf16[32,8,512]{2,1,0:T(8,128)(2,1)S(1)} async-done(((bf16[32,8,512]{2,1,0:T(8,128)(2,1)}), bf16[32,8,512]{2,1,0:T(8,128)(2,1)S(1)}, u32[]{:S(2)}, u32[]{:S(2)}) %all-to-all-start.7) | async-done | bytes 262176 | tf_op jit(solution)/shard_map/all_to_all | solution.py:48
  (140 shorter events, 51.6 us)
Async XLA Ops:
  0.6 8.0 %copy-start.3 = (bf16[256,512]{1,0:T(8,128)(2,1)S(1)}, bf16[256,512]{1,0:T(8,128)(2,1)}, u32[]{:S(2)}) copy-start(bf16[256,512]{1,0:T(8,128)(2,1)} %param.14) | copy-start | bytes 786436
  0.6 8.0 %copy-start.24 = (bf16[2,512,128]{2,1,0:T(8,128)(2,1)S(1)}, bf16[2,512,128]{2,1,0:T(8,128)(2,1)}, u32[]{:S(2)}) copy-start(bf16[2,512,128]{2,1,0:T(8,128)(2,1)} %param.17) | copy-start | bytes 786436
  3.6 12.7 %copy-start.22 = (f32[2,128]{1,0:T(2,128)S(1)}, f32[2,128]{1,0:T(2,128)}, u32[]{:S(2)}) copy-start(f32[2,128]{1,0:T(2,128)} %param.24) | copy-start | bytes 3076
  3.6 13.2 %copy-start = (f32[2,32,2,4096]{3,2,1,0:T(2,128)S(1)}, f32[2,32,2,4096]{3,2,1,0:T(2,128)}, u32[]{:S(2)}) copy-start(f32[2,32,2,4096]{3,2,1,0:T(2,128)} %param.27) | copy-start | bytes 6291460
  9.8 14.3 %all-to-all-start = ((bf16[8,32,642]{2,1,0:T(8,128)(2,1)}), bf16[8,32,642]{2,1,0:T(8,128)(2,1)S(1)}, u32[]{:S(2)}, u32[]{:S(2)}) async-start(bf16[8,32,642]{2,1,0:T(8,128)(2,1)} %concatenate.43), calls=%async_computation | async-start | bytes 786432 | tf_op jit(solution)/shard_map/all_to_all | solution.py:26
  16.9 1.2 copy-start.26
  18.0 3.2 %copy-start.23 = (f32[2,128]{1,0:T(2,128)S(1)}, f32[2,128]{1,0:T(2,128)}, u32[]{:S(2)}) copy-start(f32[2,128]{1,0:T(2,128)} %param.25) | copy-start | bytes 3076
  18.1 10.2 %copy-start.27 = (f32[32]{0:T(128)}, f32[32]{0:T(128)S(1)}, u32[]{:S(2)}) copy-start(f32[32]{0:T(128)S(1)} %fusion.99) | copy-start | bytes 388
  29.0 2.5 %copy-start.2 = (f32[32,2,64,64]{3,2,1,0:T(8,128)S(1)}, f32[32,2,64,64]{3,2,1,0:T(8,128)}, u32[]{:S(2)}) copy-start(f32[32,2,64,64]{3,2,1,0:T(8,128)} %reshape_squeeze.6) | copy-start | bytes 3145732
  29.0 2.5 %copy-start.8 = (f32[32,2,64]{2,1,0:T(2,128)S(1)}, f32[32,2,64]{2,1,0:T(2,128)}, u32[]{:S(2)}) copy-start(f32[32,2,64]{2,1,0:T(2,128)} %mul.352) | copy-start | bytes 49156
  29.0 2.5 %copy-start.17 = (f32[32,2,64,1]{2,1,0,3:T(2,128)S(1)}, f32[32,2,64,1]{2,1,0,3:T(2,128)}, u32[]{:S(2)}) copy-start(f32[32,2,64,1]{2,1,0,3:T(2,128)} %reshape.284) | copy-start | bytes 49156
  29.1 3.9 %copy-start.13 = (f32[32,2,64]{2,1,0:T(2,128)}, f32[32,2,64]{2,1,0:T(2,128)S(1)}, u32[]{:S(2)}) copy-start(f32[32,2,64]{2,1,0:T(2,128)S(1)} %get-tuple-element.4) | copy-start | bytes 49156
  31.5 25.1 %copy-start.4 = (bf16[256,512]{1,0:T(8,128)(2,1)S(1)}, bf16[256,512]{1,0:T(8,128)(2,1)}, u32[]{:S(2)}) copy-start(bf16[256,512]{1,0:T(8,128)(2,1)} %param.14) | copy-start | bytes 786436
  46.0 21.8 %all-to-all-start.2 = ((bf16[32,8,512]{2,1,0:T(8,128)(2,1)}), bf16[32,8,512]{2,1,0:T(8,128)(2,1)}, u32[]{:S(2)}, u32[]{:S(2)}) async-start(bf16[32,8,512]{2,1,0:T(8,128)(2,1)} %fusion.8), calls=%async_computation.2 | async-start | bytes 524288 | tf_op jit(solution)/shard_map/all_to_all | solution.py:26
  70.2 16.0 %copy-start.21 = (f32[1,512]{1,0:T(1,128)S(1)}, f32[1,512]{1,0:T(1,128)}, u32[]{:S(2)}) copy-start(f32[1,512]{1,0:T(1,128)} %get-tuple-element.18) | copy-start | bytes 6148
  70.2 15.3 %all-to-all-start.3 = ((bf16[32,8,512]{2,1,0:T(8,128)(2,1)}), bf16[32,8,512]{2,1,0:T(8,128)(2,1)S(1)}, u32[]{:S(2)}, u32[]{:S(2)}) async-start(bf16[32,8,512]{2,1,0:T(8,128)(2,1)} %broadcast_in_dim.9), calls=%async_computation.3 | async-start | bytes 524288 | tf_op jit(solution)/shard_map/all_to_all | solution.py:48
  77.6 13.2 %copy-start.25 = (bf16[2,512,128]{2,1,0:T(8,128)(2,1)S(1)}, bf16[2,512,128]{2,1,0:T(8,128)(2,1)}, u32[]{:S(2)}) copy-start(bf16[2,512,128]{2,1,0:T(8,128)(2,1)} %param.17) | copy-start | bytes 786436
  86.2 13.4 %copy-start.9 = (f32[32,2,64]{2,1,0:T(2,128)S(1)}, f32[32,2,64]{2,1,0:T(2,128)}, u32[]{:S(2)}) copy-start(f32[32,2,64]{2,1,0:T(2,128)} %mul.352) | copy-start | bytes 49156
  91.9 21.9 %all-to-all-start.4 = ((bf16[8,32,642]{2,1,0:T(8,128)(2,1)}), bf16[8,32,642]{2,1,0:T(8,128)(2,1)}, u32[]{:S(2)}, u32[]{:S(2)}) async-start(bf16[8,32,642]{2,1,0:T(8,128)(2,1)} %concatenate.51), calls=%async_computation.4 | async-start | bytes 786432 | tf_op jit(solution)/shard_map/all_to_all | solution.py:26
  105.5 3.2 %copy-start.14 = (f32[32,2,64]{2,1,0:T(2,128)S(1)}, f32[32,2,64]{2,1,0:T(2,128)}, u32[]{:S(2)}) copy-start(f32[32,2,64]{2,1,0:T(2,128)} %copy-done.13) | copy-start | bytes 49156
  122.7 3.3 %copy-start.1 = (f32[32,2,64,64]{3,2,1,0:T(8,128)S(1)}, f32[32,2,64,64]{3,2,1,0:T(8,128)}, u32[]{:S(2)}) copy-start(f32[32,2,64,64]{3,2,1,0:T(8,128)} %reshape_squeeze.7) | copy-start | bytes 3145732
  122.7 3.3 %copy-start.10 = (f32[32,2,64]{2,1,0:T(2,128)S(1)}, f32[32,2,64]{2,1,0:T(2,128)}, u32[]{:S(2)}) copy-start(f32[32,2,64]{2,1,0:T(2,128)} %mul.372) | copy-start | bytes 49156
  122.7 3.3 %copy-start.12 = (f32[32,2,64]{2,1,0:T(2,128)S(1)}, f32[32,2,64]{2,1,0:T(2,128)}, u32[]{:S(2)}) copy-start(f32[32,2,64]{2,1,0:T(2,128)} %mul.384) | copy-start | bytes 49156
  122.7 3.3 %copy-start.18 = (f32[32,2,64,1]{2,1,0,3:T(2,128)S(1)}, f32[32,2,64,1]{2,1,0,3:T(2,128)}, u32[]{:S(2)}) copy-start(f32[32,2,64,1]{2,1,0,3:T(2,128)} %reshape.288) | copy-start | bytes 49156
  123.7 4.4 %copy-start.15 = (f32[32,2,64]{2,1,0:T(2,128)}, f32[32,2,64]{2,1,0:T(2,128)S(1)}, u32[]{:S(2)}) copy-start(f32[32,2,64]{2,1,0:T(2,128)S(1)} %get-tuple-element.2) | copy-start | bytes 49156
  125.9 2.1 %copy-start.6 = (f32[32,2,1,64]{3,2,1,0:T(1,128)}, f32[32,2,1,64]{3,2,1,0:T(1,128)S(1)}, u32[]{:S(2)}) copy-start(f32[32,2,1,64]{3,2,1,0:T(1,128)S(1)} %fusion.105) | copy-start | bytes 49156
  133.6 9.7 %all-to-all-start.5 = ((bf16[8,32,128]{2,1,0:T(8,128)(2,1)}), bf16[8,32,128]{2,1,0:T(8,128)(2,1)S(1)}, u32[]{:S(2)}, u32[]{:S(2)}) async-start(bf16[8,32,128]{2,1,0:T(8,128)(2,1)} %broadcast_in_dim.10), calls=%async_computation.5 | async-start | bytes 131072 | tf_op jit(solution)/shard_map/all_to_all | solution.py:48
  145.1 19.7 %all-to-all-start.6 = ((bf16[32,8,512]{2,1,0:T(8,128)(2,1)}), bf16[32,8,512]{2,1,0:T(8,128)(2,1)S(1)}, u32[]{:S(2)}, u32[]{:S(2)}) async-start(bf16[32,8,512]{2,1,0:T(8,128)(2,1)} %fusion.9), calls=%async_computation.6 | async-start | bytes 524288 | tf_op jit(solution)/shard_map/all_to_all | solution.py:26
  151.9 3.2 %copy-start.7 = (f32[32,2,1,64]{3,2,1,0:T(1,128)S(1)}, f32[32,2,1,64]{3,2,1,0:T(1,128)}, u32[]{:S(2)}) copy-start(f32[32,2,1,64]{3,2,1,0:T(1,128)} %copy-done.6) | copy-start | bytes 49156
  151.9 3.2 %copy-start.16 = (f32[32,2,64]{2,1,0:T(2,128)S(1)}, f32[32,2,64]{2,1,0:T(2,128)}, u32[]{:S(2)}) copy-start(f32[32,2,64]{2,1,0:T(2,128)} %copy-done.15) | copy-start | bytes 49156
  157.0 3.2 %copy-start.11 = (f32[32,2,64]{2,1,0:T(2,128)S(1)}, f32[32,2,64]{2,1,0:T(2,128)}, u32[]{:S(2)}) copy-start(f32[32,2,64]{2,1,0:T(2,128)} %mul.372) | copy-start | bytes 49156
  166.3 19.6 %all-to-all-start.7 = ((bf16[32,8,512]{2,1,0:T(8,128)(2,1)}), bf16[32,8,512]{2,1,0:T(8,128)(2,1)S(1)}, u32[]{:S(2)}, u32[]{:S(2)}) async-start(bf16[32,8,512]{2,1,0:T(8,128)(2,1)} %broadcast_in_dim.11), calls=%async_computation.7 | async-start | bytes 524288 | tf_op jit(solution)/shard_map/all_to_all | solution.py:48
  (3 other events, 1.9 us)
where the time goes:
time: 190 us; the launch traced here: 187 us
  starting transfers between devices  47.6 us (25%)
  local copies, waits for them, and re-layouts  44.8 us (24%)
  other arithmetic  30.9 us (16%)
  waiting for transfers between devices  27.8 us (15%)
  matrix products  26 us (14%)
  blocking collectives  8.44 us (4%)
    all_to_all x4, starting transfers between devices, summed_on_arrival(): lax.all_to_all(tiles, axis, split_axis=0, concat_axis=0, tiled=True)  28.9 us
    all_to_all x3, starting transfers between devices, sent_to_all(): lax.all_to_all(jnp.broadcast_to(array[None], (count, *array.shape)), axis...  18.7 us
    all_to_all x3, waiting for transfers between devices, sent_to_all(): lax.all_to_all(jnp.broadcast_to(array[None], (count, *array.shape)), axis...  15.2 us
    all_to_all x4, waiting for transfers between devices, summed_on_arrival(): lax.all_to_all(tiles, axis, split_axis=0, concat_axis=0, tiled=True)  12.6 us
    mul x6, local copies, waits for them, and re-layouts, recur_heads(): matrix * heads_of(decay)[:, :, None, :]  10.8 us
    dot_general x10, matrix products, truncated_product(): jnp.dot(rescaled_rows, weight, preferred_element_type=jnp.float32)  9.9 us
    all_to_all x1, blocking collectives, sent_to_all(): lax.all_to_all(jnp.broadcast_to(array[None], (count, *array.shape)), axis...  8.44 us
    mul x4, local copies, waits for them, and re-layouts, recur_heads(): heads_of(value_proj)[..., None] * keys[:, :, None, :]  6.99 us
  transfers between devices with their start and end apart: 7, of which 5 were waited for; matrix products, arithmetic and copies ran while one was open for 25% of the time, Pallas kernels for 0%

commit v1 on v0

v1 whole, which is shorter than its diff:
```python
import jax
import jax.numpy as jnp
from jax import lax
from jax.experimental import pallas as pl
from jax.experimental.pallas import tpu as pltpu
from jax.sharding import PartitionSpec as P

MODEL_WIDTH = 4096
HEAD = 64
ADAPTER_RANK = 64
SPAN = 64
BLOCKS = 2
NORM_EPS = 0.25
GROUP_EPS = 0.25

N_Y, N_CORE, N_Z, N_X = 4, 2, 8, 4
N_DP, N_TP = N_Y * N_CORE, N_Z * N_X
BATCH = 256
SEQS = BATCH // N_DP
ROWS = BATCH // N_TP
FEATS = MODEL_WIDTH // N_DP
WIDTH = MODEL_WIDTH // N_TP
PAIRS = SEQS * HEAD
WIDE = 4 * WIDTH + 2 * ADAPTER_RANK

F32, BF16 = jnp.float32, jnp.bfloat16
MESH = pl.DeviceIdType.MESH
EXACT = lax.Precision.HIGHEST

DP_STEPS = [(dy, dc) for dy in (2, 1, 3) for dc in (0, 1)] + [(0, 1)]
TP_STEPS = sorted(
    [(dz, dx) for dz in range(N_Z) for dx in range(N_X) if (dz, dx) != (0, 0)],
    key=lambda s: -(min(s[0], N_Z - s[0]) + min(s[1], N_X - s[1])),
)


def stable_sigmoid(x):
    e = jnp.exp(-jnp.abs(x))
    return jnp.where(x >= 0, 1.0, e) / (1.0 + e)


def iota(shape, dim):
    return lax.broadcasted_iota(jnp.int32, shape, dim)


def kernel(
    hist, gain, decay_off, head_gain, stream_in,
    qw, kw, vw, gw, aw, du, ru, ow, state_in,
    stream_out, state_out,
    w_all, w_low, w_out, state, part, part_in, sq, sq_in, mixed, mixed_in, osum, osum_in, rows, stream_mid,
    load_sem, state_sem, send_sem, recv_sem,
):
    me_t, me_d = lax.axis_index("tp"), lax.axis_index("dp")
    z, x = me_t // N_X, me_t % N_X
    y, core = me_d // N_CORE, me_d % N_CORE
    dp_peers = [((y + dy) % N_Y) * N_CORE + (core + dc) % N_CORE for dy, dc in DP_STEPS]
    tp_peers = [((z + dz) % N_Z) * N_X + (x + dx) % N_X for dz, dx in TP_STEPS]

    barrier = pltpu.get_barrier_semaphore()
    for p in tp_peers:
        pl.semaphore_signal(barrier, inc=1, device_id={"tp": p}, device_id_type=MESH)
    for p in dp_peers:
        pl.semaphore_signal(barrier, inc=1, device_id={"dp": p}, device_id_type=MESH)

    loads = []
    for l in range(BLOCKS):
        pairs = [
            (w.at[l], w_all.at[l, :, pl.ds(i * WIDTH, WIDTH)]) for i, w in enumerate((qw, kw, vw, gw, aw))
        ]
        pairs += [
            (du.at[l], w_low.at[l, pl.ds(0, 64), pl.ds(0, WIDTH)]),
            (ru.at[l], w_low.at[l, pl.ds(64, 64), pl.ds(WIDTH, WIDTH)]),
            (ow.at[l], w_out.at[l]),
            (state_in.at[l], state.at[l]),
        ]
        loads.append([pltpu.make_async_copy(s, d, load_sem.at[l, i]) for i, (s, d) in enumerate(pairs)])
    for c in loads[0]:
        c.start()
    for c in loads[1]:
        c.start()
    for l in range(BLOCKS):
        w_low[l, pl.ds(0, 64), pl.ds(WIDTH, WIDTH)] = jnp.zeros((64, WIDTH), F32)
        w_low[l, pl.ds(64, 64), pl.ds(0, WIDTH)] = jnp.zeros((64, WIDTH), F32)

    low_lane = iota((SEQS, WIDTH), 1) < HEAD
    seg = ((iota((WIDTH, WIDTH), 0) // HEAD) == (iota((WIDTH, WIDTH), 1) // HEAD)).astype(F32)
    fold = ((iota((WIDTH, WIDTH), 0) // HEAD) == (iota((WIDTH, WIDTH), 1) % 2)).astype(F32).astype(BF16)
    spread = ((iota((WIDTH, WIDTH), 1) // HEAD) == (iota((WIDTH, WIDTH), 0) % 2)).astype(F32).astype(BF16)
    r_i, l_i = iota((HEAD, WIDTH), 0), iota((HEAD, WIDTH), 1)
    pick = ((l_i // HEAD == r_i % 2) & ((l_i % HEAD) // 2 == r_i // 2)).astype(F32)
    even_row = (iota((SEQS, 8, WIDTH), 1) % 2) == 0
    eye = iota((128, 128), 0) == iota((128, 128), 1)
    mine = iota((SEQS, BATCH), 1) == iota((SEQS, BATCH), 0) + me_d * SEQS

    pos = jnp.zeros((SEQS, WIDTH), F32)
    seq_i = iota((SEQS, WIDTH), 0)
    for i in range(SEQS):
        pos = jnp.where(seq_i == i, 0.5 + ((hist[i] // SPAN) % 3).astype(F32), pos)

    def per_row(v):
        r = pltpu.roll(v, HEAD, 1)
        t0, t1 = jnp.where(low_lane, v, r), jnp.where(low_lane, r, v)
        return jnp.where(even_row, t0[:, None, :], t1[:, None, :])

    def split_dot(v, m):
        hi = v.astype(BF16)
        lo = (v - hi.astype(F32)).astype(BF16)
        return jnp.dot(hi, m, preferred_element_type=F32) + jnp.dot(lo, m, preferred_element_type=F32)

    def send(src, dst, l, s, peer):
        pltpu.make_async_remote_copy(
            src_ref=src, dst_ref=dst, send_sem=send_sem.at[l, s], recv_sem=recv_sem.at[l, s],
            device_id=peer, device_id_type=MESH,
        ).start()

    def wait_bytes(ref, sem):
        pltpu.make_async_copy(ref, ref, sem).wait()

    for l in range(BLOCKS):
        stream = stream_in if l == 0 else stream_mid.at[l - 1]
        xf = stream[...].astype(F32).reshape(BATCH, FEATS)
        sq_col = jnp.sum(xf * xf, axis=1, keepdims=True)
        for i in range(BATCH // 128):
            sq[l, :, pl.ds(i * 128, 128)] = jnp.sum(
                jnp.where(eye, sq_col[i * 128 : (i + 1) * 128], 0.0), axis=0, keepdims=True
            )
        scaled = (xf * gain[pl.ds(l, 1), :]).astype(BF16)
        for c in loads[l][:5]:
            c.wait()
        product = jnp.dot(scaled, w_all[l], preferred_element_type=F32)
        part[l] = product.astype(BF16).reshape(N_DP, SEQS, WIDE)
        if l == 0:
            pl.semaphore_wait(barrier, len(tp_peers) + len(dp_peers))
        for p in dp_peers:
            send(part.at[l, p], part_in.at[l, me_d], l, 0, {"dp": p})
        for p in dp_peers:
            send(sq.at[l], sq_in.at[l, me_d], l, 1, {"dp": p})
        part_in[l, me_d] = part[l, me_d]
        sq_in[l, me_d] = sq[l]
        for c in loads[l][5:]:
            c.wait()

        wait_bytes(sq_in.at[l, pl.ds(0, N_DP - 1)], recv_sem.at[l, 1])
        sq_all = sq_in[l, 0]
        for d in range(1, N_DP):
            sq_all = sq_all + sq_in[l, d]
        own_sq = jnp.sum(jnp.where(mine, sq_all, 0.0), axis=1, keepdims=True)
        inv = lax.rsqrt(own_sq / MODEL_WIDTH + NORM_EPS)
        wait_bytes(part_in.at[l, pl.ds(0, N_DP - 1)], recv_sem.at[l, 0])
        total = part_in[l, 0].astype(F32)
        for d in range(1, N_DP):
            total = total + part_in[l, d].astype(F32)
        total = total * inv
        query, key, value, gate, low = [total[:, i * WIDTH : (i + 1) * WIDTH] for i in range(5)]

        low = jnp.where(low_lane, jnp.tanh(low), low)
        up = jnp.dot(low, w_low[l], preferred_element_type=F32, precision=EXACT)
        decay = jnp.exp(
            -(stable_sigmoid(decay_off[pl.ds(l, 1), :] + up[:, :WIDTH]) * 0.6065306597126334) * pos
        )
        learn = stable_sigmoid(up[:, WIDTH:])
        sums = jnp.dot(
            jnp.concatenate([key * key, key * learn * query, key * query], axis=0), seg,
            preferred_element_type=F32, precision=EXACT,
        )
        key_inv = lax.rsqrt(sums[:SEQS] + 1.0)
        key_unit = key * key_inv
        key_rate = key_unit * learn
        rate_query, key_query = sums[SEQS : 2 * SEQS] * key_inv, sums[2 * SEQS :]

        unit_rows, query_rows = per_row(key_unit), per_row(decay * query)
        got = []
        for rows8 in (unit_rows, query_rows):
            prod = state[l].reshape(SEQS, HEAD // 8, 8, WIDTH) * rows8[:, None]
            folded = split_dot(prod.reshape(PAIRS, WIDTH), fold).reshape(SEQS, HEAD, WIDTH)
            got.append(jnp.sum(folded * pick[None], axis=1))
        state_key, state_query = got
        readout = state_query - state_key * rate_query + value * key_query
        mean = jnp.dot(readout, seg, preferred_element_type=F32, precision=EXACT) * (1.0 / HEAD)
        centred = readout - mean
        var = jnp.dot(centred * centred, seg, preferred_element_type=F32, precision=EXACT) * (1.0 / HEAD)
        normed = centred * lax.rsqrt(var + GROUP_EPS) * head_gain[pl.ds(l, 1), :]
        own_mixed = (normed * stable_sigmoid(gate)).astype(BF16)
        mixed[l] = own_mixed
        for p in dp_peers:
            send(mixed.at[l], mixed_in.at[l, me_d], l, 2, {"dp": p})
        mixed_in[l, me_d] = own_mixed

        def outer(v):
            return split_dot((v[:, None, :] * pick[None]).reshape(PAIRS, WIDTH), spread).reshape(
                SEQS, HEAD // 8, 8, WIDTH
            )

        state[l] = (
            state[l].reshape(SEQS, HEAD // 8, 8, WIDTH) * per_row(decay)[:, None]
            - outer(state_key) * per_row(key_rate)[:, None]
            + outer(value) * per_row(key)[:, None]
        ).reshape(PAIRS, WIDTH)
        pltpu.make_async_copy(state.at[l], state_out.at[l], state_sem.at[l]).start()

        wait_bytes(mixed_in.at[l, pl.ds(0, N_DP - 1)], recv_sem.at[l, 2])
        out_part = jnp.dot(mixed_in[l].reshape(BATCH, WIDTH), w_out[l], preferred_element_type=F32)
        osum[l] = out_part.reshape(N_TP, ROWS, FEATS).astype(BF16)
        for p in tp_peers:
            send(osum.at[l, p], osum_in.at[l, me_t], l, 3, {"tp": p})
        osum_in[l, me_t] = osum[l, me_t]
        wait_bytes(osum_in.at[l, pl.ds(0, N_TP - 1)], recv_sem.at[l, 3])
        new = stream[me_t].astype(F32) + jnp.sum(osum_in[l].astype(F32), axis=0)
        rows[l] = new.astype(BF16)
        for p in tp_peers:
            send(rows.at[l], stream_mid.at[l, me_t], l, 4, {"tp": p})
        stream_mid[l, me_t] = rows[l]
        wait_bytes(stream_mid.at[l, pl.ds(0, N_TP - 1)], recv_sem.at[l, 4])

    stream_out[...] = stream_mid[BLOCKS - 1]
    for l in range(BLOCKS):
        pltpu.make_async_copy(state.at[l], state_out.at[l], state_sem.at[l]).wait()
        wait_bytes(part.at[l, pl.ds(0, N_DP - 1)], send_sem.at[l, 0])
        wait_bytes(sq_in.at[l, pl.ds(0, N_DP - 1)], send_sem.at[l, 1])
        wait_bytes(mixed_in.at[l, pl.ds(0, N_DP - 1)], send_sem.at[l, 2])
        wait_bytes(osum.at[l, pl.ds(0, N_TP - 1)], send_sem.at[l, 3])
        wait_bytes(stream_mid.at[l, pl.ds(0, N_TP - 1)], send_sem.at[l, 4])


def body(
    stream, history, input_norm_gain, query_weight, key_weight, value_weight, gate_weight, adapter_down_weight,
    decay_up_weight, rate_up_weight, decay_offset, head_norm_gain, output_weight, recurrent_state,
):
    state = recurrent_state.reshape(BLOCKS, SEQS, 2, HEAD // 2, WIDTH).transpose(0, 1, 3, 2, 4)
    state = state.reshape(BLOCKS, PAIRS, WIDTH)
    vmem, anywhere = pl.BlockSpec(memory_space=pltpu.VMEM), pl.BlockSpec(memory_space=pl.ANY)
    new_stream, new_state = pl.pallas_call(
        kernel,
        out_shape=(
            jax.ShapeDtypeStruct((N_TP, ROWS, FEATS), BF16),
            jax.ShapeDtypeStruct((BLOCKS, PAIRS, WIDTH), F32),
        ),
        in_specs=[pl.BlockSpec(memory_space=pltpu.SMEM), vmem, vmem, vmem, vmem] + [anywhere] * 9,
        out_specs=(vmem, anywhere),
        scratch_shapes=[
            pltpu.VMEM((BLOCKS, FEATS, WIDE), BF16),
            pltpu.VMEM((BLOCKS, 2 * ADAPTER_RANK, 2 * WIDTH), F32),
            pltpu.VMEM((BLOCKS, WIDTH, FEATS), BF16),
            pltpu.VMEM((BLOCKS, PAIRS, WIDTH), F32),
            pltpu.VMEM((BLOCKS, N_DP, SEQS, WIDE), BF16),
            pltpu.VMEM((BLOCKS, N_DP, SEQS, WIDE), BF16),
            pltpu.VMEM((BLOCKS, 1, BATCH), F32),
            pltpu.VMEM((BLOCKS, N_DP, 1, BATCH), F32),
            pltpu.VMEM((BLOCKS, SEQS, WIDTH), BF16),
            pltpu.VMEM((BLOCKS, N_DP, SEQS, WIDTH), BF16),
            pltpu.VMEM((BLOCKS, N_TP, ROWS, FEATS), BF16),
            pltpu.VMEM((BLOCKS, N_TP, ROWS, FEATS), BF16),
            pltpu.VMEM((BLOCKS, ROWS, FEATS), BF16),
            pltpu.VMEM((BLOCKS, N_TP, ROWS, FEATS), BF16),
            pltpu.SemaphoreType.DMA((BLOCKS, 9)),
            pltpu.SemaphoreType.DMA((BLOCKS,)),
            pltpu.SemaphoreType.DMA((BLOCKS, 5)),
            pltpu.SemaphoreType.DMA((BLOCKS, 5)),
        ],
        compiler_params=pltpu.CompilerParams(collective_id=0, has_side_effects=True),
        name="two_blocks",
    )(
        history, input_norm_gain, decay_offset, head_norm_gain, stream.reshape(N_TP, ROWS, FEATS),
        query_weight, key_weight, value_weight, gate_weight, adapter_down_weight,
        decay_up_weight, rate_up_weight, output_weight, state,
    )
    new_state = new_state.reshape(BLOCKS, SEQS, HEAD // 2, 2, WIDTH).transpose(0, 1, 3, 2, 4)
    return new_stream.reshape(BATCH, FEATS), new_state.reshape(BLOCKS, SEQS, 2, HEAD * HEAD)


def solution(mesh):
    placed = (
        P(None, "dp"), P("dp"), P(None, "dp"),
        P(None, "dp", "tp"), P(None, "dp", "tp"), P(None, "dp", "tp"), P(None, "dp", "tp"),
        P(None, "dp", None), P(None, None, "tp"), P(None, None, "tp"), P(None, "tp"), P(None, "tp"),
        P(None, "tp", "dp"), P(None, "dp", "tp", None),
    )
    return jax.shard_map(
        body,
        mesh=mesh,
        in_specs=placed,
        out_specs=(P(None, "dp"), P(None, "dp", "tp", None)),
        check_vma=False,
    )
```

time: 190 us -> 75.3 us (0.40); the launches traced: 187 us -> 75.1 us
  Pallas kernels: 0 us -> 69.7 us
  starting transfers between devices: 47.6 us -> 0 us
  local copies, waits for them, and re-layouts: 44.8 us -> 4.83 us
  other arithmetic: 30.9 us -> 0 us
  waiting for transfers between devices: 27.8 us -> 0 us
  matrix products: 26 us -> 0 us
  blocking collectives: 8.44 us -> 0 us
    pallas_call x0 -> x1, Pallas kernels: none -> 69.7 us  [body(): pl.pallas_call(kernel, out_shape=(jax.ShapeDtypeStruct((N_TP, ROWS, FEATS...]
    all_to_all x7 -> x0, starting transfers between devices: 47.6 us -> none  [the longest x4 28.9 us: summed_on_arrival(): lax.all_to_all(tiles, axis, split_axis=0, concat_axis=0, tiled=True)]
    all_to_all x7 -> x0, waiting for transfers between devices: 27.8 us -> none  [the longest x3 15.2 us: sent_to_all(): lax.all_to_all(jnp.broadcast_to(array[None], (count, *array.shape)), axis...]
    dot_general x20 -> x0, matrix products: 26 us -> none  [the longest x10 9.9 us: truncated_product(): jnp.dot(rescaled_rows, weight, preferred_element_type=jnp.float32)]
    mul x13 -> x0, local copies, waits for them, and re-layouts: 24.7 us -> none  [the longest x6 10.8 us: recur_heads(): matrix * heads_of(decay)[:, :, None, :]]
    mul x10 -> x0, other arithmetic: 12.6 us -> none  [the longest x2 4.63 us: recur_heads(): heads_of(value_proj)[..., None] * keys[:, :, None, :]]
    all_to_all x1 -> x0, blocking collectives: 8.44 us -> none  [sent_to_all(): lax.all_to_all(jnp.broadcast_to(array[None], (count, *array.shape)), axis...]
    reduce_sum x12 -> x0, other arithmetic: 5.74 us -> none  [the longest x4 2.17 us: summed_on_arrival(): return arrived.astype(jnp.float32).sum(axis=0)]
  transfers between devices with their start and end apart: 7 -> 0, of which waited for: 5 -> 0; matrix products, arithmetic and copies ran while one was open for 25% -> 0% of each run, Pallas kernels for 0% -> 0%
where the time goes in v1:
time: 75.3 us; the launch traced here: 75.1 us
  Pallas kernels  69.7 us (93%)
  local copies, waits for them, and re-layouts  4.83 us (6%)
    pallas_call x1, Pallas kernels, body(): pl.pallas_call(kernel, out_shape=(jax.ShapeDtypeStruct((N_TP, ROWS, FEATS...  69.7 us
    unnamed x2, local copies, waits for them, and re-layouts  4.83 us

profile of v1, /device:TPU:1, one launch (start us, length us, event | category | flops | bytes accessed | tf_op | source)
XLA Modules:
  0.0 75.1 jit_solution(14879093253457788380)
XLA Ops:
  0.6 69.7 %two_blocks.1 = (bf16[32,8,512]{2,1,0:T(8,128)(2,1)}, f32[2,2048,128]{2,1,0:T(8,128)}) custom-call(s32[32]{0:T(128)} %hist.1, f32[2,512]{1,0:T(2,128)} %gain.1, f32[2,128]{1,0:T(2,128)} %decay_off.1, f32[2,128]{1,0:T(2,128)} %head_gain.1, bf16[32,8,512]{2,1,0:T(8,128)(2,1)} %bitcast.14, bf16[2,512,128]{2,1,0:T(8,128)(2,1)} %qw.1, bf16[2,512,128]{2,1,0:T(8,128)(2,1)} %kw.1, ...), custom_call_target="tpu_custom_call" | custom-call | tf_op jit(solution)/shard_map/two_blocks/pallas_call | solution.py:232
  70.3 1.7 %copy.20 = bf16[256,512]{1,0:T(8,128)(2,1)} copy(bf16[256,512]{1,0:T(8,128)(2,1)} %bitcast.15) | data formatting | bytes 524288
  72.0 3.2 %copy.21 = f32[2,32,2,4096]{3,2,1,0:T(2,128)} copy(f32[2,32,2,4096]{3,2,1,0:T(2,128)} %bitcast.13) | data formatting | bytes 4194304

commit v2 on v1

v2 whole, which is shorter than its diff:
```python
import jax
import jax.numpy as jnp
from jax import lax
from jax.experimental import pallas as pl
from jax.experimental.pallas import tpu as pltpu
from jax.sharding import PartitionSpec as P

MODEL_WIDTH = 4096
HEAD = 64
ADAPTER_RANK = 64
SPAN = 64
BLOCKS = 2
NORM_EPS = 0.25
GROUP_EPS = 0.25

N_Y, N_CORE, N_Z, N_X = 4, 2, 8, 4
N_DP, N_TP = N_Y * N_CORE, N_Z * N_X
BATCH = 256
SEQS = BATCH // N_DP
ROWS = BATCH // N_TP
FEATS = MODEL_WIDTH // N_DP
WIDTH = MODEL_WIDTH // N_TP
PAIRS = SEQS * HEAD
WIDE = 4 * WIDTH + 2 * ADAPTER_RANK

F32, BF16 = jnp.float32, jnp.bfloat16
MESH = pl.DeviceIdType.MESH
EXACT = lax.Precision.HIGHEST

def hops(step, size):
    return min(step, size - step)


DP_STEPS = [(dy, dc) for dy in (2, 1, 3) for dc in (0, 1)] + [(0, 1)]
Z_STEPS = [4, 3, 5, 2, 6, 1, 7]
X_STEPS = [2, 1, 3]
SLAB_STEPS = sorted(
    [(dx, dy, dc) for dx in range(N_X) for dy in range(N_Y) for dc in range(N_CORE) if (dx, dy, dc) != (0, 0, 0)],
    key=lambda s: -(hops(s[0], N_X) + hops(s[1], N_Y)),
)


def stable_sigmoid(x):
    e = jnp.exp(-jnp.abs(x))
    return jnp.where(x >= 0, 1.0, e) / (1.0 + e)


def iota(shape, dim):
    return lax.broadcasted_iota(jnp.int32, shape, dim)


def kernel(
    hist_in, gain_in, decay_off_in, head_gain_in, stream_in, qw, kw, vw, gw, aw, du, ru, ow, state_in,
    stream_out, state_out,
    hist, gain, decay_off, head_gain, first, w_all, w_low, w_out, state,
    part, part_in, sq, sq_in, mixed, mixed_in, osum, osum_in, rows, stream_mid,
    load_sem, misc_sem, send_sem, recv_sem, ring_sem,
):
    me_t, me_d = lax.axis_index("tp"), lax.axis_index("dp")
    z, x = me_t // N_X, me_t % N_X
    y, core = me_d // N_CORE, me_d % N_CORE
    dp_peers = [((y + dy) % N_Y) * N_CORE + (core + dc) % N_CORE for dy, dc in DP_STEPS]
    z_peers = [(dz, (z + dz) % N_Z) for dz in Z_STEPS]
    x_peers = [(x + dx) % N_X for dx in X_STEPS]
    slab_peers = [
        ((x + dx) % N_X, ((y + dy) % N_Y) * N_CORE + (core + dc) % N_CORE) for dx, dy, dc in SLAB_STEPS
    ]

    barrier = pltpu.get_barrier_semaphore()
    for px, pd in slab_peers:
        pl.semaphore_signal(barrier, inc=1, device_id={"tp": z * N_X + px, "dp": pd}, device_id_type=MESH)
    for _, p in z_peers:
        pl.semaphore_signal(barrier, inc=1, device_id={"tp": p * N_X + x}, device_id_type=MESH)

    def start(src, dst, sem):
        c = pltpu.make_async_copy(src, dst, sem)
        c.start()
        return c

    first_loads = [start(stream_in, first, misc_sem.at[0]), start(gain_in, gain, misc_sem.at[1])]
    weight_loads, small_loads, state_loads = [], [], []
    for l in range(BLOCKS):
        weight_loads.append([
            start(w.at[l], w_all.at[l, :, pl.ds(i * WIDTH, WIDTH)], load_sem.at[l, i])
            for i, w in enumerate((qw, kw, vw, gw, aw))
        ])
        small_loads.append([
            start(du.at[l], w_low.at[l, pl.ds(0, 64), pl.ds(0, WIDTH)], load_sem.at[l, 5]),
            start(ru.at[l], w_low.at[l, pl.ds(64, 64), pl.ds(WIDTH, WIDTH)], load_sem.at[l, 6]),
            start(ow.at[l], w_out.at[l, x], load_sem.at[l, 7]),
        ])
        if l == 0:
            small_loads[0] += [
                start(hist_in, hist, misc_sem.at[2]),
                start(decay_off_in, decay_off, misc_sem.at[3]),
                start(head_gain_in, head_gain, misc_sem.at[4]),
            ]
        state_loads.append(start(state_in.at[l], state.at[l], load_sem.at[l, 8]))

    def send(src, dst, l, s, peer, sem=None):
        pltpu.make_async_remote_copy(
            src_ref=src, dst_ref=dst, send_sem=send_sem.at[l, s],
            recv_sem=recv_sem.at[l, s] if sem is None else sem,
            device_id=peer, device_id_type=MESH,
        ).start()

    def wait_bytes(ref, sem):
        pltpu.make_async_copy(ref, ref, sem).wait()

    def per_row(v):
        r = pltpu.roll(v, HEAD, 1)
        t0, t1 = jnp.where(low_lane, v, r), jnp.where(low_lane, r, v)
        return jnp.where(even_row, t0[:, None, :], t1[:, None, :])

    def split_dot(v, m):
        hi = v.astype(BF16)
        lo = (v - hi.astype(F32)).astype(BF16)
        return jnp.dot(hi, m, preferred_element_type=F32) + jnp.dot(lo, m, preferred_element_type=F32)

    eye = iota((128, 128), 0) == iota((128, 128), 1)
    for l in range(BLOCKS):
        with jax.named_scope("project"):
            if l == 0:
                for c in first_loads:
                    c.wait()
            stream = first if l == 0 else stream_mid
            xf = stream[...].astype(F32).reshape(BATCH, FEATS)
            sq_col = jnp.sum(xf * xf, axis=1, keepdims=True)
            for i in range(BATCH // 128):
                sq[l, :, pl.ds(i * 128, 128)] = jnp.sum(
                    jnp.where(eye, sq_col[i * 128 : (i + 1) * 128], 0.0), axis=0, keepdims=True
                )
            scaled = (xf * gain[pl.ds(l, 1), :]).astype(BF16)
            for c in weight_loads[l]:
                c.wait()
            product = jnp.dot(scaled, w_all[l], preferred_element_type=F32)
            part[l] = product.astype(BF16).reshape(N_DP, SEQS, WIDE)
        with jax.named_scope("barrier"):
            if l == 0:
                pl.semaphore_wait(barrier, len(slab_peers) + len(z_peers))
        with jax.named_scope("send_part"):
            for p in dp_peers:
                send(part.at[l, p], part_in.at[l, me_d], l, 0, {"dp": p})
            for p in dp_peers:
                send(sq.at[l], sq_in.at[l, me_d], l, 1, {"dp": p})
            part_in[l, me_d] = part[l, me_d]
            sq_in[l, me_d] = sq[l]
            for p in x_peers:
                send(ow.at[l], w_out.at[l, x], l, 5, {"tp": z * N_X + p})
            for c in small_loads[l]:
                c.wait()
            w_low[l, pl.ds(0, 64), pl.ds(WIDTH, WIDTH)] = jnp.zeros((64, WIDTH), F32)
            w_low[l, pl.ds(64, 64), pl.ds(0, WIDTH)] = jnp.zeros((64, WIDTH), F32)
            if l == 0:
                low_lane = iota((SEQS, WIDTH), 1) < HEAD
                seg = ((iota((WIDTH, WIDTH), 0) // HEAD) == (iota((WIDTH, WIDTH), 1) // HEAD)).astype(F32)
                half, parity = iota((WIDTH, WIDTH), 0) // HEAD, iota((WIDTH, WIDTH), 1) % 2
                fold = (half == parity).astype(F32).astype(BF16)
                half, parity = iota((WIDTH, WIDTH), 1) // HEAD, iota((WIDTH, WIDTH), 0) % 2
                spread = (half == parity).astype(F32).astype(BF16)
                r_i, l_i = iota((HEAD, WIDTH), 0), iota((HEAD, WIDTH), 1)
                pick = ((l_i // HEAD == r_i % 2) & ((l_i % HEAD) // 2 == r_i // 2)).astype(F32)
                even_row = (iota((SEQS, 8, WIDTH), 1) % 2) == 0
                mine = iota((SEQS, BATCH), 1) == iota((SEQS, BATCH), 0) + me_d * SEQS
                pos = jnp.zeros((SEQS, WIDTH), F32)
                seq_i = iota((SEQS, WIDTH), 0)
                for i in range(SEQS):
                    pos = jnp.where(seq_i == i, 0.5 + ((hist[i] // SPAN) % 3).astype(F32), pos)
            state_loads[l].wait()
        with jax.named_scope("wait_part"):
            wait_bytes(sq_in.at[l, pl.ds(0, N_DP - 1)], recv_sem.at[l, 1])
            sq_all = sq_in[l, 0]
            for d in range(1, N_DP):
                sq_all = sq_all + sq_in[l, d]
            own_sq = jnp.sum(jnp.where(mine, sq_all, 0.0), axis=1, keepdims=True)
            inv = lax.rsqrt(own_sq / MODEL_WIDTH + NORM_EPS)
            wait_bytes(part_in.at[l, pl.ds(0, N_DP - 1)], recv_sem.at[l, 0])
        with jax.named_scope("recur"):
            total = part_in[l, 0].astype(F32)
            for d in range(1, N_DP):
                total = total + part_in[l, d].astype(F32)
            total = total * inv
            query, key, value, gate, low = [total[:, i * WIDTH : (i + 1) * WIDTH] for i in range(5)]

            low = jnp.where(low_lane, jnp.tanh(low), low)
            up = jnp.dot(low, w_low[l], preferred_element_type=F32, precision=EXACT)
            decay = jnp.exp(
                -(stable_sigmoid(decay_off[pl.ds(l, 1), :] + up[:, :WIDTH]) * 0.6065306597126334) * pos
            )
            learn = stable_sigmoid(up[:, WIDTH:])
            sums = jnp.dot(
                jnp.concatenate([key * key, key * learn * query, key * query], axis=0), seg,
                preferred_element_type=F32, precision=EXACT,
            )
            key_inv = lax.rsqrt(sums[:SEQS] + 1.0)
            key_unit = key * key_inv
            key_rate = key_unit * learn
            rate_query, key_query = sums[SEQS : 2 * SEQS] * key_inv, sums[2 * SEQS :]

            unit_rows, query_rows = per_row(key_unit), per_row(decay * query)
            got = []
            for rows8 in (unit_rows, query_rows):
                prod = state[l].reshape(SEQS, HEAD // 8, 8, WIDTH) * rows8[:, None]
                folded = split_dot(prod.reshape(PAIRS, WIDTH), fold).reshape(SEQS, HEAD, WIDTH)
                got.append(jnp.sum(folded * pick[None], axis=1))
            state_key, state_query = got
            readout = state_query - state_key * rate_query + value * key_query
            mean = jnp.dot(readout, seg, preferred_element_type=F32, precision=EXACT) * (1.0 / HEAD)
            centred = readout - mean
            var = jnp.dot(centred * centred, seg, preferred_element_type=F32, precision=EXACT) * (1.0 / HEAD)
            normed = centred * lax.rsqrt(var + GROUP_EPS) * head_gain[pl.ds(l, 1), :]
            own_mixed = (normed * stable_sigmoid(gate)).astype(BF16)
        with jax.named_scope("send_mixed"):
            own_mixed = own_mixed.reshape(N_X, ROWS, WIDTH)
            mixed[l] = own_mixed
            for px, pd in slab_peers:
                send(mixed.at[l, px], mixed_in.at[l, x * N_DP + me_d], l, 2, {"tp": z * N_X + px, "dp": pd})
            mixed_in[l, x * N_DP + me_d] = mixed[l, x]
        with jax.named_scope("update"):

            def outer(v):
                return split_dot((v[:, None, :] * pick[None]).reshape(PAIRS, WIDTH), spread).reshape(
                    SEQS, HEAD // 8, 8, WIDTH
                )

            state_out[l] = (
                state[l].reshape(SEQS, HEAD // 8, 8, WIDTH) * per_row(decay)[:, None]
                - outer(state_key) * per_row(key_rate)[:, None]
                + outer(value) * per_row(key)[:, None]
            ).reshape(PAIRS, WIDTH)
        with jax.named_scope("wait_mixed"):
            wait_bytes(w_out.at[l, pl.ds(0, N_X - 1)], recv_sem.at[l, 5])
            wait_bytes(mixed_in.at[l, pl.ds(0, len(slab_peers))], recv_sem.at[l, 2])
        with jax.named_scope("output"):
            out_part = jnp.zeros((N_DP * ROWS, FEATS), F32)
            for i in range(N_X):
                out_part = out_part + jnp.dot(
                    mixed_in[l, pl.ds(i * N_DP, N_DP)].reshape(N_DP * ROWS, WIDTH), w_out[l, i], preferred_element_type=F32
                )
            osum[l] = out_part.reshape(N_Z, ROWS, FEATS).astype(BF16)
            for _, p in z_peers:
                send(osum.at[l, p], osum_in.at[l, z], l, 3, {"tp": p * N_X + x})
            osum_in[l, z] = osum[l, z]
        with jax.named_scope("wait_sum"):
            wait_bytes(osum_in.at[l, pl.ds(0, N_Z - 1)], recv_sem.at[l, 3])
        with jax.named_scope("send_rows"):
            own = first[me_t] if l == 0 else rows[0]
            new = own.astype(F32) + jnp.sum(osum_in[l].astype(F32), axis=0)
            rows[l] = new.astype(BF16)
            target = stream_mid if l == 0 else stream_out
            for dz, p in z_peers:
                send(rows.at[l], target.at[me_t], l, 4, {"tp": p * N_X + x}, sem=ring_sem.at[l, dz])
            for p in x_peers:
                send(rows.at[l], target.at[me_t], l, 4, {"tp": z * N_X + p})
            target[me_t] = rows[l]
        with jax.named_scope("wait_rows"):
            for dz in Z_STEPS[::-1]:
                src = (z + N_Z - dz) % N_Z * N_X + x
                wait_bytes(target.at[0], ring_sem.at[l, dz])
                for p in x_peers:
                    send(target.at[src], target.at[src], l, 4, {"tp": z * N_X + p})
            wait_bytes(target.at[pl.ds(0, N_TP - N_Z)], recv_sem.at[l, 4])

    with jax.named_scope("drain"):
        for l in range(BLOCKS):
            wait_bytes(part.at[l, pl.ds(0, N_DP - 1)], send_sem.at[l, 0])
            wait_bytes(sq_in.at[l, pl.ds(0, N_DP - 1)], send_sem.at[l, 1])
            wait_bytes(mixed_in.at[l, pl.ds(0, len(slab_peers))], send_sem.at[l, 2])
            wait_bytes(osum.at[l, pl.ds(0, N_Z - 1)], send_sem.at[l, 3])
            wait_bytes(stream_mid.at[pl.ds(0, N_TP - 1)], send_sem.at[l, 4])
            wait_bytes(w_out.at[l, pl.ds(0, N_X - 1)], send_sem.at[l, 5])


def put(stream_in, state_in, stream_out, state_out, sem):
    copies = [
        pltpu.make_async_copy(state_in, state_out, sem.at[0]),
        pltpu.make_async_copy(stream_in, stream_out, sem.at[1]),
    ]
    for c in copies:
        c.start()
    for c in copies:
        c.wait()


def body(
    stream, history, input_norm_gain, query_weight, key_weight, value_weight, gate_weight, adapter_down_weight,
    decay_up_weight, rate_up_weight, decay_offset, head_norm_gain, output_weight, recurrent_state,
):
    state = recurrent_state.reshape(BLOCKS, SEQS, 2, HEAD // 2, WIDTH).transpose(0, 1, 3, 2, 4)
    state = state.reshape(BLOCKS, PAIRS, WIDTH)
    vmem, hbm = pl.BlockSpec(memory_space=pltpu.VMEM), pl.BlockSpec(memory_space=pltpu.HBM)
    stream_shape, state_shape = (N_TP, ROWS, FEATS), (BLOCKS, PAIRS, WIDTH)
    new_stream, new_state = pl.pallas_call(
        kernel,
        out_shape=(pltpu.VMEM(stream_shape, BF16), pltpu.VMEM(state_shape, F32)),
        in_specs=[hbm] * 14,
        out_specs=(vmem, vmem),
        scratch_shapes=[
            pltpu.SMEM((SEQS,), jnp.int32),
            pltpu.VMEM((BLOCKS, FEATS), F32),
            pltpu.VMEM((BLOCKS, WIDTH), F32),
            pltpu.VMEM((BLOCKS, WIDTH), F32),
            pltpu.VMEM(stream_shape, BF16),
            pltpu.VMEM((BLOCKS, FEATS, WIDE), BF16),
            pltpu.VMEM((BLOCKS, 2 * ADAPTER_RANK, 2 * WIDTH), F32),
            pltpu.VMEM((BLOCKS, N_X, WIDTH, FEATS), BF16),
            pltpu.VMEM(state_shape, F32),
            pltpu.VMEM((BLOCKS, N_DP, SEQS, WIDE), BF16),
            pltpu.VMEM((BLOCKS, N_DP, SEQS, WIDE), BF16),
            pltpu.VMEM((BLOCKS, 1, BATCH), F32),
            pltpu.VMEM((BLOCKS, N_DP, 1, BATCH), F32),
            pltpu.VMEM((BLOCKS, N_X, ROWS, WIDTH), BF16),
            pltpu.VMEM((BLOCKS, N_X * N_DP, ROWS, WIDTH), BF16),
            pltpu.VMEM((BLOCKS, N_Z, ROWS, FEATS), BF16),
            pltpu.VMEM((BLOCKS, N_Z, ROWS, FEATS), BF16),
            pltpu.VMEM((BLOCKS, ROWS, FEATS), BF16),
            pltpu.VMEM(stream_shape, BF16),
            pltpu.SemaphoreType.DMA((BLOCKS, 9)),
            pltpu.SemaphoreType.DMA((5,)),
            pltpu.SemaphoreType.DMA((BLOCKS, 6)),
            pltpu.SemaphoreType.DMA((BLOCKS, 6)),
            pltpu.SemaphoreType.DMA((BLOCKS, N_Z)),
        ],
        compiler_params=pltpu.CompilerParams(
            collective_id=0, has_side_effects=True, vmem_limit_bytes=64684032
        ),
        name="two_blocks",
    )(
        history, input_norm_gain, decay_offset, head_norm_gain, stream.reshape(stream_shape),
        query_weight, key_weight, value_weight, gate_weight, adapter_down_weight,
        decay_up_weight, rate_up_weight, output_weight, state,
    )
    new_stream, new_state = pl.pallas_call(
        put,
        out_shape=(jax.ShapeDtypeStruct(stream_shape, BF16), jax.ShapeDtypeStruct(state_shape, F32)),
        in_specs=[vmem, vmem],
        out_specs=(hbm, hbm),
        scratch_shapes=[pltpu.SemaphoreType.DMA((2,))],
        compiler_params=pltpu.CompilerParams(vmem_limit_bytes=2**20),
        name="put",
    )(new_stream, new_state)
    new_state = new_state.reshape(BLOCKS, SEQS, HEAD // 2, 2, WIDTH).transpose(0, 1, 3, 2, 4)
    return new_stream.reshape(BATCH, FEATS), new_state.reshape(BLOCKS, SEQS, 2, HEAD * HEAD)


def solution(mesh):
    placed = (
        P(None, "dp"), P("dp"), P(None, "dp"),
        P(None, "dp", "tp"), P(None, "dp", "tp"), P(None, "dp", "tp"), P(None, "dp", "tp"),
        P(None, "dp", None), P(None, None, "tp"), P(None, None, "tp"), P(None, "tp"), P(None, "tp"),
        P(None, "tp", "dp"), P(None, "dp", "tp", None),
    )
    return jax.shard_map(
        body,
        mesh=mesh,
        in_specs=placed,
        out_specs=(P(None, "dp"), P(None, "dp", "tp", None)),
        check_vma=False,
    )
```

time: 75.3 us -> 62.2 us (0.83); the launches traced: 75.1 us -> 61.3 us
  Pallas kernels: 69.7 us -> 60.6 us
  local copies, waits for them, and re-layouts: 4.83 us -> 0 us
    pallas_call x1 -> x2, Pallas kernels: 69.7 us -> 60.6 us  [the longest x1 59.2 us: body(): pl.pallas_call(kernel, out_shape=(pltpu.VMEM(stream_shape, BF16), pltpu.V...]
    unnamed x2 -> x0, local copies, waits for them, and re-layouts: 4.83 us -> none
where the time goes in v2:
time: 62.2 us; the launch traced here: 61.3 us
  Pallas kernels  60.6 us (97%)
  between operations  0.64 us (1%)
    pallas_call x1, Pallas kernels, body(): pl.pallas_call(kernel, out_shape=(pltpu.VMEM(stream_shape, BF16), pltpu.V...  59.2 us
    pallas_call x1, Pallas kernels, body(): pl.pallas_call(put, out_shape=(jax.ShapeDtypeStruct(stream_shape, BF16),...  1.41 us

profile of v2, /device:TPU:1, one launch (start us, length us, event | category | flops | bytes accessed | tf_op | source)
XLA Modules:
  0.0 61.3 jit_solution(12040192529822217317)
XLA Ops:
  0.6 59.2 %two_blocks.1 = (bf16[32,8,512]{2,1,0:T(8,128)(2,1)S(1)}, f32[2,2048,128]{2,1,0:T(8,128)S(1)}) custom-call(s32[32]{0:T(128)} %hist_in.1, f32[2,512]{1,0:T(2,128)} %gain_in.1, f32[2,128]{1,0:T(2,128)} %decay_off_in.1, f32[2,128]{1,0:T(2,128)} %head_gain_in.1, bf16[32,8,512]{2,1,0:T(8,128)(2,1)} %bitcast.13, bf16[2,512,128]{2,1,0:T(8,128)(2,1)} %qw.1, ...), custom_call_target="tpu_custom_call" | custom-call | tf_op jit(solution)/shard_map/two_blocks/pallas_call | solution.py:293
  59.8 1.4 %put.1 = (bf16[32,8,512]{2,1,0:T(8,128)(2,1)}, f32[2,2048,128]{2,1,0:T(8,128)}) custom-call(bf16[32,8,512]{2,1,0:T(8,128)(2,1)S(1)} %get-tuple-element.6.stream_in, f32[2,2048,128]{2,1,0:T(8,128)S(1)} %get-tuple-element.7.state_in), custom_call_target="tpu_custom_call" | custom-call | tf_op jit(solution)/shard_map/put/pallas_call | solution.py:333

commit v3 on v2

v3 whole, which is shorter than its diff:
```python
import jax
import jax.numpy as jnp
from jax import lax
from jax.experimental import pallas as pl
from jax.experimental.pallas import tpu as pltpu
from jax.sharding import PartitionSpec as P

MODEL_WIDTH = 4096
HEAD = 64
ADAPTER_RANK = 64
SPAN = 64
BLOCKS = 2
NORM_EPS = 0.25
GROUP_EPS = 0.25

N_Y, N_CORE, N_Z, N_X = 4, 2, 8, 4
N_DP, N_TP = N_Y * N_CORE, N_Z * N_X
BATCH = 256
SEQS = BATCH // N_DP
ROWS = BATCH // N_TP
FEATS = MODEL_WIDTH // N_DP
WIDTH = MODEL_WIDTH // N_TP
PAIRS = SEQS * HEAD
WIDE = 4 * WIDTH + 2 * ADAPTER_RANK

F32, BF16 = jnp.float32, jnp.bfloat16
MESH = pl.DeviceIdType.MESH

def hops(step, size):
    return min(step, size - step)


DP_STEPS = [(dy, dc) for dy in (2, 1, 3) for dc in (0, 1)] + [(0, 1)]
Y_STEPS = [2, 1, 3]
Z_STEPS = [4, 3, 5, 2, 6, 1, 7]
X_STEPS = [2, 1, 3]
SLAB_STEPS = sorted(
    [(dx, dy, dc) for dx in range(N_X) for dy in range(N_Y) for dc in range(N_CORE) if (dx, dy, dc) != (0, 0, 0)],
    key=lambda s: -(hops(s[0], N_X) + hops(s[1], N_Y)),
)
FORWARD = {1: (2, 1, 3), 7: (2, 1, 3), 2: (2, 1, 3), 6: (2, 1, 3), 3: (1, 3), 5: (1, 3)}
ROW_STEPS = [(3, 0), (5, 0), (2, 0), (6, 0), (4, 2), (4, 1), (4, 3), (3, 2), (5, 2), (4, 0), (1, 0), (7, 0)]
ROW_STEPS += [(0, 2), (0, 1), (0, 3)]


def stable_sigmoid(x):
    e = jnp.exp(-jnp.abs(x))
    return jnp.where(x >= 0, 1.0, e) / (1.0 + e)


def iota(shape, dim):
    return lax.broadcasted_iota(jnp.int32, shape, dim)


def kernel(
    hist_in, gain_in, decay_off_in, head_gain_in, stream_in, qw, kw, vw, gw, aw, du, ru, ow, state_in,
    stream_out, state_out,
    hist, gains, decay_off, head_gain, first, w_first, w_second, low_raw, w_low, w_out, state,
    part0, part0_in, part1, part1_in, sq0, sq0_in, sq1, sq1_in, mixed, mixed_in, osum, osum_in, rows, stream_mid,
    load_sem, misc_sem, send_sem, recv_sem, ring_sem,
):
    me_t, me_d = lax.axis_index("tp"), lax.axis_index("dp")
    z, x = me_t // N_X, me_t % N_X
    y, core = me_d // N_CORE, me_d % N_CORE
    dp_peers = [((y + dy) % N_Y) * N_CORE + (core + dc) % N_CORE for dy, dc in DP_STEPS]
    y_peers = [(y + dy) % N_Y for dy in Y_STEPS]
    z_peers = [(dz, (z + dz) % N_Z) for dz in Z_STEPS]
    x_peers = [(x + dx) % N_X for dx in X_STEPS]
    slab_peers = [
        ((x + dx) % N_X, ((y + dy) % N_Y) * N_CORE + (core + dc) % N_CORE) for dx, dy, dc in SLAB_STEPS
    ]
    partner = y * N_CORE + (core + 1) % N_CORE

    def start(src, dst, sem):
        c = pltpu.make_async_copy(src, dst, sem)
        c.start()
        return c

    def load_weights(l, dst):
        return [
            start(w.at[l], dst.at[:, pl.ds(i * WIDTH, WIDTH)], load_sem.at[l, i])
            for i, w in enumerate((qw, kw, vw, gw, aw))
        ]

    def load_small(l):
        return [
            start(du.at[l], low_raw.at[l, 0], load_sem.at[l, 5]),
            start(ru.at[l], low_raw.at[l, 1], load_sem.at[l, 6]),
            start(ow.at[l], w_out.at[l, x], load_sem.at[l, 7]),
        ]

    def load_state(l):
        return start(state_in.at[l], state.at[l], load_sem.at[l, 8])

    first_loads = [start(stream_in, first, misc_sem.at[0]), start(gain_in, gains.at[core], misc_sem.at[1])]
    weight_loads = load_weights(0, w_first)

    barrier = pltpu.get_barrier_semaphore()
    for px, pd in slab_peers:
        pl.semaphore_signal(barrier, inc=1, device_id={"tp": z * N_X + px, "dp": pd}, device_id_type=MESH)
    for _, p in z_peers:
        pl.semaphore_signal(barrier, inc=1, device_id={"tp": p * N_X + x}, device_id_type=MESH)

    def send(src, dst, l, s, peer, sem=None):
        pltpu.make_async_remote_copy(
            src_ref=src, dst_ref=dst, send_sem=send_sem.at[l, s],
            recv_sem=recv_sem.at[l, s] if sem is None else sem,
            device_id=peer, device_id_type=MESH,
        ).start()

    def wait_bytes(ref, sem):
        pltpu.make_async_copy(ref, ref, sem).wait()

    def halves(v):
        hi = v.astype(BF16)
        return hi, (v - hi.astype(F32)).astype(BF16)

    def split_dot(v, m):
        hi, lo = halves(v)
        return jnp.dot(hi, m, preferred_element_type=F32) + jnp.dot(lo, m, preferred_element_type=F32)

    def same(shape, group_a, group_b):
        return (group_a(iota(shape, 0)) == group_b(iota(shape, 1))).astype(F32).astype(BF16)

    eye = iota((128, 128), 0) == iota((128, 128), 1)

    def squares(xs):
        col = sum(jnp.sum(v * v, axis=1, keepdims=True) for v in xs)
        return [
            jnp.sum(jnp.where(eye, col[i : i + 128], 0.0), axis=0, keepdims=True) for i in range(0, col.shape[0], 128)
        ]

    for l in range(BLOCKS):
        with jax.named_scope("project"):
            if l == 0:
                for c in first_loads:
                    c.wait()
                xs = [first[...].astype(F32).reshape(BATCH, FEATS)]
                scaled = (xs[0] * gains[core, pl.ds(0, 1), :]).astype(BF16)
                for c in weight_loads:
                    c.wait()
                product = jnp.dot(scaled, w_first[...], preferred_element_type=F32)
                part0[...] = product.astype(BF16).reshape(N_DP, SEQS, WIDE)
                small_loads = load_small(0) + [
                    start(hist_in, hist, misc_sem.at[2]),
                    start(decay_off_in, decay_off, misc_sem.at[3]),
                    start(head_gain_in, head_gain, misc_sem.at[4]),
                ]
                state_load = load_state(0)
            else:
                half = N_TP // N_CORE
                xs = [
                    stream_mid[pl.ds(c * half, half)].astype(F32).reshape(BATCH // N_CORE, FEATS)
                    for c in range(N_CORE)
                ]
                product = sum(
                    jnp.dot(
                        (xs[c] * gains[c, pl.ds(1, 1), :]).astype(BF16), w_second[c], preferred_element_type=F32
                    )
                    for c in range(N_CORE)
                )
                part1[...] = product.astype(BF16).reshape(N_Y, SEQS, WIDE)
        with jax.named_scope("barrier"):
            if l == 0:
                pl.semaphore_wait(barrier, len(slab_peers) + len(z_peers))
        with jax.named_scope("send_part"):
            if l == 0:
                for p in dp_peers:
                    send(part0.at[p], part0_in.at[me_d], l, 0, {"dp": p})
                for i, v in enumerate(squares(xs)):
                    sq0[:, pl.ds(i * 128, 128)] = v
                for p in dp_peers:
                    send(sq0, sq0_in.at[me_d], l, 1, {"dp": p})
                part0_in[me_d] = part0[me_d]
                sq0_in[me_d] = sq0[...]
            else:
                for p in y_peers:
                    send(part1.at[p], part1_in.at[y], l, 0, {"dp": p * N_CORE + core})
                sq1[...] = squares(xs)[0]
                for p in y_peers:
                    send(sq1, sq1_in.at[y], l, 1, {"dp": p * N_CORE + core})
                part1_in[y] = part1[y]
                sq1_in[y] = sq1[...]
            for p in x_peers:
                send(ow.at[l], w_out.at[l, x], l, 5, {"tp": z * N_X + p})
            if l == 0:
                send(gains.at[core], gains.at[core], l, 6, {"dp": partner})
                next_weights = load_weights(1, w_second.at[core])
            for c in small_loads:
                c.wait()
            none = jnp.zeros((ADAPTER_RANK, WIDTH), F32)
            up_hi, up_lo = halves(jnp.concatenate([
                jnp.concatenate([low_raw[l, 0], none], axis=1), jnp.concatenate([none, low_raw[l, 1]], axis=1)
            ], axis=0))
            w_low[l] = jnp.concatenate([up_hi, up_hi, up_lo], axis=0)
            if l == 0:
                low_lane = iota((SEQS, WIDTH), 1) < HEAD
                head = lambda i: i % WIDTH // HEAD
                seg = same((2 * WIDTH, WIDTH), head, head)
                fold = same((2 * WIDTH, 2 * WIDTH), lambda i: i // HEAD, lambda i: i // WIDTH * 2 + i % 2)
                spread = same((WIDTH, WIDTH), lambda i: i % 2, head)
                r_i, l_i = iota((HEAD, WIDTH), 0), iota((HEAD, WIDTH), 1)
                pick = ((l_i // HEAD == r_i % 2) & ((l_i % HEAD) // 2 == r_i // 2)).astype(F32)
                even_row = (iota((SEQS, 8, WIDTH), 1) % 2) == 0
                pos = jnp.zeros((SEQS, WIDTH), F32)
                seq_i = iota((SEQS, WIDTH), 0)
                for i in range(SEQS):
                    pos = jnp.where(seq_i == i, 0.5 + ((hist[i] // SPAN) % 3).astype(F32), pos)
            state_load.wait()
        with jax.named_scope("wait_part"):
            part_in, sq_in = (part0_in, sq0_in) if l == 0 else (part1_in, sq1_in)
            count, place = (N_DP, me_d) if l == 0 else (N_Y, y)
            wait_bytes(sq_in.at[pl.ds(0, count - 1)], recv_sem.at[l, 1])
            sq_all = sq_in[0]
            for d in range(1, count):
                sq_all = sq_all + sq_in[d]
            shape = (SEQS, count * SEQS)
            mine = iota(shape, 1) == iota(shape, 0) + place * SEQS
            own_sq = jnp.sum(jnp.where(mine, sq_all, 0.0), axis=1, keepdims=True)
            inv = lax.rsqrt(own_sq / MODEL_WIDTH + NORM_EPS)
            wait_bytes(part_in.at[pl.ds(0, count - 1)], recv_sem.at[l, 0])
        with jax.named_scope("recur"):
            total = part_in[0].astype(F32)
            for d in range(1, count):
                total = total + part_in[d].astype(F32)
            total = total * inv
            query, key, value, gate, low = [total[:, i * WIDTH : (i + 1) * WIDTH] for i in range(5)]

            def seg_dot(v):
                return jnp.dot(jnp.concatenate(halves(v), axis=1), seg, preferred_element_type=F32)

            def per_row(v):
                r = pltpu.roll(v, HEAD, 1)
                t0, t1 = jnp.where(low_lane, v, r), jnp.where(low_lane, r, v)
                return jnp.where(even_row, t0[:, None, :], t1[:, None, :])

            low_hi, low_lo = halves(jnp.where(low_lane, jnp.tanh(low), low))
            up = jnp.dot(
                jnp.concatenate([low_hi, low_lo, low_hi], axis=1), w_low[l], preferred_element_type=F32
            )
            decay = jnp.exp(
                -(stable_sigmoid(decay_off[pl.ds(l, 1), :] + up[:, :WIDTH]) * 0.6065306597126334) * pos
            )
            learn = stable_sigmoid(up[:, WIDTH:])
            sums = seg_dot(jnp.concatenate([key * key, key * learn * query, key * query], axis=0))
            key_inv = lax.rsqrt(sums[:SEQS] + 1.0)
            key_unit = key * key_inv
            key_rate = key_unit * learn
            rate_query, key_query = sums[SEQS : 2 * SEQS] * key_inv, sums[2 * SEQS :]

            held = state[l].reshape(SEQS, HEAD // 8, 8, WIDTH)
            prods = jnp.concatenate([
                (held * per_row(v)[:, None]).reshape(PAIRS, WIDTH) for v in (key_unit, decay * query)
            ], axis=1)
            folded = split_dot(prods, fold).reshape(SEQS, HEAD, 2 * WIDTH)
            state_key = jnp.sum(folded[:, :, :WIDTH] * pick[None], axis=1)
            state_query = jnp.sum(folded[:, :, WIDTH:] * pick[None], axis=1)
            readout = state_query - state_key * rate_query + value * key_query
            centred = readout - seg_dot(readout) * (1.0 / HEAD)
            var = seg_dot(centred * centred) * (1.0 / HEAD)
            normed = centred * lax.rsqrt(var + GROUP_EPS) * head_gain[pl.ds(l, 1), :]
            own_mixed = (normed * stable_sigmoid(gate)).astype(BF16)
        with jax.named_scope("send_mixed"):
            mixed[l] = own_mixed.reshape(N_X, ROWS, WIDTH)
            for px, pd in slab_peers:
                send(mixed.at[l, px], mixed_in.at[l, x * N_DP + me_d], l, 2, {"tp": z * N_X + px, "dp": pd})
            mixed_in[l, x * N_DP + me_d] = mixed[l, x]
        with jax.named_scope("update"):
            if l == 0:
                for c in next_weights:
                    c.wait()
                send(w_second.at[core], w_second.at[core], l, 7, {"dp": partner})
                small_loads = load_small(1)
                state_load = load_state(1)

            def outer(v):
                return split_dot((v[:, None, :] * pick[None]).reshape(PAIRS, WIDTH), spread).reshape(
                    SEQS, HEAD // 8, 8, WIDTH
                )

            state_out[l] = (
                held * per_row(decay)[:, None]
                - outer(state_key) * per_row(key_rate)[:, None]
                + outer(value) * per_row(key)[:, None]
            ).reshape(PAIRS, WIDTH)
        with jax.named_scope("wait_mixed"):
            wait_bytes(w_out.at[l, pl.ds(0, N_X - 1)], recv_sem.at[l, 5])
            wait_bytes(mixed_in.at[l, pl.ds(0, len(slab_peers))], recv_sem.at[l, 2])
        with jax.named_scope("output"):
            out_part = jnp.zeros((N_DP * ROWS, FEATS), F32)
            for i in range(N_X):
                out_part = out_part + jnp.dot(
                    mixed_in[l, pl.ds(i * N_DP, N_DP)].reshape(N_DP * ROWS, WIDTH), w_out[l, i],
                    preferred_element_type=F32,
                )
            osum[l] = out_part.reshape(N_Z, ROWS, FEATS).astype(BF16)
            for _, p in z_peers:
                send(osum.at[l, p], osum_in.at[l, z], l, 3, {"tp": p * N_X + x})
            osum_in[l, z] = osum[l, z]
        with jax.named_scope("wait_sum"):
            wait_bytes(osum_in.at[l, pl.ds(0, N_Z - 1)], recv_sem.at[l, 3])
        with jax.named_scope("send_rows"):
            own = first[me_t] if l == 0 else rows[0]
            new = own.astype(F32) + jnp.sum(osum_in[l].astype(F32), axis=0)
            rows[l] = new.astype(BF16)
            if l == 0:
                target, row_d = stream_mid, y * N_CORE + z % N_CORE
                place = lambda pz, c: c * (N_TP // N_CORE) + pz // N_CORE * N_X + x
            else:
                target, row_d = stream_out, me_d
                place = lambda pz, c: pz * N_X + x
            here = place(z, core)
            for dz, dx in ROW_STEPS:
                send(
                    rows.at[l], target.at[here], l, 4,
                    {"tp": (z + dz) % N_Z * N_X + (x + dx) % N_X, "dp": row_d},
                    sem=ring_sem.at[l, dz, core] if dx == 0 and dz in FORWARD else None,
                )

            def pass_on(dz, c):
                there = place((z + N_Z - dz) % N_Z, c)
                wait_bytes(target.at[0], ring_sem.at[l, dz, c])
                for dx in FORWARD[dz]:
                    pltpu.make_async_remote_copy(
                        src_ref=target.at[there], dst_ref=target.at[there], send_sem=send_sem.at[1, 6 + l],
                        recv_sem=recv_sem.at[l, 4], device_id={"tp": z * N_X + (x + dx) % N_X}, device_id_type=MESH,
                    ).start()

        with jax.named_scope("wait_rows"):
            if l == 0:
                even = (z + core) % 2 == 0

                @pl.when(even)
                def _():
                    target[here] = rows[l]
                    for dz in (2, 6):
                        for c in range(N_CORE):
                            pass_on(dz, c)
                    wait_bytes(target.at[pl.ds(0, 27)], recv_sem.at[l, 4])

                @pl.when(jnp.logical_not(even))
                def _():
                    pltpu.make_async_remote_copy(
                        src_ref=rows.at[l], dst_ref=target.at[here], send_sem=send_sem.at[1, 8],
                        recv_sem=recv_sem.at[l, 4], device_id={"dp": partner}, device_id_type=MESH,
                    ).start()
                    for dz in (1, 7, 3, 5):
                        for c in range(N_CORE):
                            pass_on(dz, c)
                    wait_bytes(target.at[pl.ds(0, 24)], recv_sem.at[l, 4])

                wait_bytes(gains.at[0], recv_sem.at[l, 6])
                wait_bytes(w_second.at[0], recv_sem.at[l, 7])
            else:
                target[here] = rows[l]
                for dz in (1, 7, 2, 6, 3, 5):
                    pass_on(dz, core)
                wait_bytes(target.at[pl.ds(0, 25)], recv_sem.at[l, 4])

    with jax.named_scope("drain"):
        wait_bytes(part0.at[pl.ds(0, N_DP - 1)], send_sem.at[0, 0])
        wait_bytes(sq0_in.at[pl.ds(0, N_DP - 1)], send_sem.at[0, 1])
        wait_bytes(part1.at[pl.ds(0, N_Y - 1)], send_sem.at[1, 0])
        wait_bytes(sq1_in.at[pl.ds(0, N_Y - 1)], send_sem.at[1, 1])
        wait_bytes(gains.at[0], send_sem.at[0, 6])
        wait_bytes(w_second.at[0], send_sem.at[0, 7])
        for l in range(BLOCKS):
            wait_bytes(mixed_in.at[l, pl.ds(0, len(slab_peers))], send_sem.at[l, 2])
            wait_bytes(osum.at[l, pl.ds(0, N_Z - 1)], send_sem.at[l, 3])
            wait_bytes(stream_mid.at[pl.ds(0, len(ROW_STEPS))], send_sem.at[l, 4])
            wait_bytes(w_out.at[l, pl.ds(0, N_X - 1)], send_sem.at[l, 5])
        wait_bytes(stream_mid.at[pl.ds(0, 16)], send_sem.at[1, 7])

        @pl.when((z + core) % 2 == 0)
        def _():
            wait_bytes(stream_mid.at[pl.ds(0, 12)], send_sem.at[1, 6])

        @pl.when((z + core) % 2 != 0)
        def _():
            wait_bytes(stream_mid.at[pl.ds(0, 20)], send_sem.at[1, 6])
            wait_bytes(stream_mid.at[0], send_sem.at[1, 8])


def put(stream_in, state_in, stream_out, state_out, sem):
    copies = [
        pltpu.make_async_copy(state_in, state_out, sem.at[0]),
        pltpu.make_async_copy(stream_in, stream_out, sem.at[1]),
    ]
    for c in copies:
        c.start()
    for c in copies:
        c.wait()


def body(
    stream, history, input_norm_gain, query_weight, key_weight, value_weight, gate_weight, adapter_down_weight,
    decay_up_weight, rate_up_weight, decay_offset, head_norm_gain, output_weight, recurrent_state,
):
    state = recurrent_state.reshape(BLOCKS, SEQS, 2, HEAD // 2, WIDTH).transpose(0, 1, 3, 2, 4)
    state = state.reshape(BLOCKS, PAIRS, WIDTH)
    vmem, hbm = pl.BlockSpec(memory_space=pltpu.VMEM), pl.BlockSpec(memory_space=pltpu.HBM)
    stream_shape, state_shape = (N_TP, ROWS, FEATS), (BLOCKS, PAIRS, WIDTH)
    new_stream, new_state = pl.pallas_call(
        kernel,
        out_shape=(pltpu.VMEM(stream_shape, BF16), pltpu.VMEM(state_shape, F32)),
        in_specs=[hbm] * 14,
        out_specs=(vmem, vmem),
        scratch_shapes=[
            pltpu.SMEM((SEQS,), jnp.int32),
            pltpu.VMEM((N_CORE, BLOCKS, FEATS), F32),
            pltpu.VMEM((BLOCKS, WIDTH), F32),
            pltpu.VMEM((BLOCKS, WIDTH), F32),
            pltpu.VMEM(stream_shape, BF16),
            pltpu.VMEM((FEATS, WIDE), BF16),
            pltpu.VMEM((N_CORE, FEATS, WIDE), BF16),
            pltpu.VMEM((BLOCKS, 2, ADAPTER_RANK, WIDTH), F32),
            pltpu.VMEM((BLOCKS, 6 * ADAPTER_RANK, 2 * WIDTH), BF16),
            pltpu.VMEM((BLOCKS, N_X, WIDTH, FEATS), BF16),
            pltpu.VMEM(state_shape, F32),
            pltpu.VMEM((N_DP, SEQS, WIDE), BF16),
            pltpu.VMEM((N_DP, SEQS, WIDE), BF16),
            pltpu.VMEM((N_Y, SEQS, WIDE), BF16),
            pltpu.VMEM((N_Y, SEQS, WIDE), BF16),
            pltpu.VMEM((1, BATCH), F32),
            pltpu.VMEM((N_DP, 1, BATCH), F32),
            pltpu.VMEM((1, BATCH // N_CORE), F32),
            pltpu.VMEM((N_Y, 1, BATCH // N_CORE), F32),
            pltpu.VMEM((BLOCKS, N_X, ROWS, WIDTH), BF16),
            pltpu.VMEM((BLOCKS, N_X * N_DP, ROWS, WIDTH), BF16),
            pltpu.VMEM((BLOCKS, N_Z, ROWS, FEATS), BF16),
            pltpu.VMEM((BLOCKS, N_Z, ROWS, FEATS), BF16),
            pltpu.VMEM((BLOCKS, ROWS, FEATS), BF16),
            pltpu.VMEM(stream_shape, BF16),
            pltpu.SemaphoreType.DMA((BLOCKS, 9)),
            pltpu.SemaphoreType.DMA((5,)),
            pltpu.SemaphoreType.DMA((BLOCKS, 9)),
            pltpu.SemaphoreType.DMA((BLOCKS, 8)),
            pltpu.SemaphoreType.DMA((BLOCKS, N_Z, N_CORE)),
        ],
        compiler_params=pltpu.CompilerParams(
            collective_id=0, has_side_effects=True, vmem_limit_bytes=64684032
        ),
        name="two_blocks",
    )(
        history, input_norm_gain, decay_offset, head_norm_gain, stream.reshape(stream_shape),
        query_weight, key_weight, value_weight, gate_weight, adapter_down_weight,
        decay_up_weight, rate_up_weight, output_weight, state,
    )
    new_stream, new_state = pl.pallas_call(
        put,
        out_shape=(jax.ShapeDtypeStruct(stream_shape, BF16), jax.ShapeDtypeStruct(state_shape, F32)),
        in_specs=[vmem, vmem],
        out_specs=(hbm, hbm),
        scratch_shapes=[pltpu.SemaphoreType.DMA((2,))],
        compiler_params=pltpu.CompilerParams(vmem_limit_bytes=2**20),
        name="put",
    )(new_stream, new_state)
    new_state = new_state.reshape(BLOCKS, SEQS, HEAD // 2, 2, WIDTH).transpose(0, 1, 3, 2, 4)
    return new_stream.reshape(BATCH, FEATS), new_state.reshape(BLOCKS, SEQS, 2, HEAD * HEAD)


def solution(mesh):
    placed = (
        P(None, "dp"), P("dp"), P(None, "dp"),
        P(None, "dp", "tp"), P(None, "dp", "tp"), P(None, "dp", "tp"), P(None, "dp", "tp"),
        P(None, "dp", None), P(None, None, "tp"), P(None, None, "tp"), P(None, "tp"), P(None, "tp"),
        P(None, "tp", "dp"), P(None, "dp", "tp", None),
    )
    return jax.shard_map(
        body,
        mesh=mesh,
        in_specs=placed,
        out_specs=(P(None, "dp"), P(None, "dp", "tp", None)),
        check_vma=False,
    )
```

time: 62.2 us -> 63.2 us (1.016)
  Pallas kernels: 60.6 us -> 61.3 us
    pallas_call x1, Pallas kernels: 59.2 us -> 59.9 us  [body(): pl.pallas_call(kernel, out_shape=(pltpu.VMEM(stream_shape, BF16), pltpu.V...]
where the time goes in v3:
time: 63.2 us; the launch traced here: 62 us
  Pallas kernels  61.3 us (97%)
  between operations  0.64 us (1%)
    pallas_call x1, Pallas kernels, body(): pl.pallas_call(kernel, out_shape=(pltpu.VMEM(stream_shape, BF16), pltpu.V...  59.9 us
    pallas_call x1, Pallas kernels, body(): pl.pallas_call(put, out_shape=(jax.ShapeDtypeStruct(stream_shape, BF16),...  1.41 us

profile of v3, /device:TPU:1, one launch (start us, length us, event | category | flops | bytes accessed | tf_op | source)
XLA Modules:
  0.0 62.0 jit_solution(8292601930211216091)
XLA Ops:
  0.6 59.9 %two_blocks.1 = (bf16[32,8,512]{2,1,0:T(8,128)(2,1)S(1)}, f32[2,2048,128]{2,1,0:T(8,128)S(1)}) custom-call(s32[32]{0:T(128)} %hist_in.1, f32[2,512]{1,0:T(2,128)} %gain_in.1, f32[2,128]{1,0:T(2,128)} %decay_off_in.1, f32[2,128]{1,0:T(2,128)} %head_gain_in.1, bf16[32,8,512]{2,1,0:T(8,128)(2,1)} %bitcast.13, bf16[2,512,128]{2,1,0:T(8,128)(2,1)} %qw.1, ...), custom_call_target="tpu_custom_call" | custom-call | tf_op jit(solution)/shard_map/two_blocks/pallas_call | solution.py:403
  60.6 1.4 %put.1 = (bf16[32,8,512]{2,1,0:T(8,128)(2,1)}, f32[2,2048,128]{2,1,0:T(8,128)}) custom-call(bf16[32,8,512]{2,1,0:T(8,128)(2,1)S(1)} %get-tuple-element.6.stream_in, f32[2,2048,128]{2,1,0:T(8,128)S(1)} %get-tuple-element.7.state_in), custom_call_target="tpu_custom_call" | custom-call | tf_op jit(solution)/shard_map/put/pallas_call | solution.py:449
